TPU v7x, 256 devices: a whole 4x4x8 slice. The times are simulated.
256 devices in a mesh: kv: 32 (over z, x), tp: 8 (over y, core).
Axes of the slice: x: 4, y: 4, z: 8, core: 2. Of those that a mesh axis runs over, the one named last changes fastest.
Arguments:
- tokens: bfloat16 [16384, 2048], P('kv'), may hold values from -64 to 64
- query_weight: bfloat16 [2048, 2048], P(None, 'tp'), may hold values from -0.1875 to 0.1875
- chosen_key_weight: bfloat16 [2048, 512], P(None, 'tp'), may hold values from -0.125 to 0.125
- chosen_value_weight: bfloat16 [2048, 512], P(None, 'tp'), may hold values from -0.125 to 0.125
- summary_key_weight: bfloat16 [2048, 512], P(None, 'tp'), may hold values from -0.125 to 0.125
- summary_value_weight: bfloat16 [2048, 512], P(None, 'tp'), may hold values from -0.125 to 0.125
- squeeze_key_in: bfloat16 [2048, 128], replicated, may hold values from -0.125 to 0.125
- squeeze_key_out: bfloat16 [128, 64], replicated, may hold values from -1 to 1
- squeeze_value_in: bfloat16 [2048, 128], replicated, may hold values from -0.125 to 0.125
- squeeze_value_out: bfloat16 [128, 64], replicated, may hold values from -2 to 2
- gate_weight: bfloat16 [2, 2048, 32], P(None, None, 'tp'), may hold values from -0.125 to 0.125
- output_weight: bfloat16 [2048, 2048], P('tp'), may hold values from -1 to 1
- chosen_blocks: int32 [8, 512, 16], P('tp', 'kv'), may hold values from 0 to 511, as said below
Outputs:
- attended: bfloat16 [16384, 2048], P(('kv', 'tp'))
Inputs may be any that keep to these rules, and one draw needn't show every extreme that they name: `chosen_blocks`: each row lists 16 different blocks. The row of query block b lists b, lists b - 1 where b > 0, and lists block 0. Take the blocks at or below their query block that the rows of the query blocks of one index of kv list for one key head: at most 4 different ones lie among the positions of any other single index of kv, and exactly 4 among the positions of the first index, for every index after the first.
All inputs are finite; a program needn't handle non-finite values.
Results may differ from a plain program's by a relative error of at most 0.03.
Values may be sent and summed in bfloat16 or wider, within the bound.
No kernel may reach another device: no remote copies, remote signals or barrier semaphores. Data moves between devices by JAX's collectives and lax.ppermute only.
A program may use at most 128 MiB of HBM per device.

v0:
```python
import jax
import jax.numpy as jnp
import numpy as np
from jax import lax
from jax.experimental import pallas as pl
from jax.experimental.pallas import tpu as pltpu
from jax.sharding import PartitionSpec as P


HD = 64
CMP_STRIDE = 16
BLK = 32
NSEL = 16
CAP = 4
ROTARY_BASE = 10000.0
NEG = -1e30
FLOOR = -1e29
TOK = 512
PEERS = 32
NSUM = 32
ROWS = 40
QB = TOK // BLK
HEADS = 4
NBLK = PEERS * QB
UNUSED = 99.0
AT_ONCE = 4
CHIPS = 4
PER_CHIP = QB // CHIPS
CHUNKS = 2
PICK = 8
PART = 128
OUT_ROWS = TOK // 8

INVERSE = (ROTARY_BASE ** (-np.arange(HD // 2, dtype=np.float64) / (HD // 2))).astype(np.float32)
INVERSE_ROW = np.tile(INVERSE, 4)[None, :]
SIGN_ROW = np.tile(np.repeat(np.array([-1.0, 1.0], np.float32), HD // 2), 2)[None, :]

bf16 = jnp.bfloat16
f32 = jnp.float32


def dot(a, b):
    return jnp.dot(a, b, preferred_element_type=f32)


def dot_t(a, b):
    return lax.dot_general(a, b, (((1,), (1,)), ((), ())), preferred_element_type=f32)


def lanes_of(shape):
    return lax.broadcasted_iota(jnp.int32, shape, len(shape) - 1)


def rows_of(shape):
    return lax.broadcasted_iota(jnp.int32, shape, len(shape) - 2)


def turned(x, cosine, sine):
    lane = lanes_of(x.shape)
    swapped = jnp.where(lane % HD < HD // 2, pltpu.roll(x, 128 - HD // 2, 1), pltpu.roll(x, HD // 2, 1))
    return x * cosine + swapped * sine


def gelu(x):
    return 0.5 * x * (1.0 + jnp.tanh(np.float32(np.sqrt(2.0 / np.pi)) * (x + 0.044715 * (x * x * x))))


def squeeze_out(pre_k, pre_v, out_k, out_v, cosine, sine):
    hidden = jnp.concatenate([gelu(pre_k).astype(bf16), gelu(pre_v).astype(bf16)], 1)
    zero = jnp.zeros(out_k.shape, bf16)
    weight = jnp.concatenate(
        [jnp.concatenate([out_k, zero], 1), jnp.concatenate([zero, out_v], 1)], 0
    )
    both = dot_t(hidden, weight)
    return jnp.where(lanes_of(both.shape) < HD, turned(both, cosine, sine), both)


def summary_kernel(
    rank_ref, tokens_hbm, wk_hbm, wv_hbm, ink_hbm, inv_hbm, outk_hbm, outv_hbm, turn_hbm, chosen_hbm,
    payload_ref, code_ref,
    tokens_ref, weight_ref, ink_ref, inv_ref, outk_ref, outv_ref, turn_ref, chosen_ref, raw_ref, sems,
):
    rank = rank_ref[0]
    part = TOK // CHUNKS
    copies = [
        (chosen_hbm, chosen_ref),
        (wk_hbm, weight_ref.at[:HD]),
        (wv_hbm, weight_ref.at[HD:]),
        *((tokens_hbm.at[pl.ds(c * part, part)], tokens_ref.at[pl.ds(c * part, part)]) for c in range(CHUNKS)),
        (ink_hbm, ink_ref),
        (inv_hbm, inv_ref),
        (outk_hbm, outk_ref),
        (outv_hbm, outv_ref),
        (turn_hbm, turn_ref),
    ]
    copies = [pltpu.make_async_copy(a, b, sems.at[n]) for n, (a, b) in enumerate(copies)]
    for copy in copies:
        copy.start()
    copies[0].wait()
    chosen = chosen_ref[...]
    query_block = rank * QB + rows_of(chosen.shape)
    wanted = jnp.where((chosen <= query_block) & (chosen // QB != rank), chosen, -1)
    every = lanes_of((QB, NBLK))
    hit = jnp.zeros((QB, NBLK), f32)
    for k in range(NSEL):
        hit = jnp.where(every == wanted[:, k : k + 1], 1.0, hit)
    present = jnp.broadcast_to(jnp.max(hit, 0, keepdims=True), (8, NBLK))
    lane = lanes_of((8, NBLK))
    running = present
    for step in (1, 2, 4, 8):
        running = running + jnp.where(lane % QB >= step, pltpu.roll(running, step, 1), 0.0)
    code = jnp.where(present > 0.0, running - present, UNUSED)
    code_ref[...] = code
    copies[1].wait()
    copies[2].wait()
    for c in range(CHUNKS):
        copies[3 + c].wait()
        rows = slice(c * part, c * part + part)
        raw_ref[rows] = dot_t(tokens_ref[rows], weight_ref[...]).astype(bf16).astype(f32)
    for copy in copies[3 + CHUNKS :]:
        copy.wait()
    ends = (rank * NSUM + rows_of((NSUM, 128))) * CMP_STRIDE + 2 * CMP_STRIDE - 1
    angles = ends.astype(f32) * turn_ref[:1]
    cosine = jnp.cos(angles)
    sine = jnp.sin(angles) * turn_ref[1:]
    zero = jnp.zeros((HD, 128), bf16)
    total = jnp.zeros((NSUM, 512), f32)
    for p in range(0, CMP_STRIDE, 2):
        left = []
        right = []
        for q in (p, p + 1):
            left.append(raw_ref[pl.ds(q, NSUM, stride=CMP_STRIDE), :].astype(bf16))
            low = pl.ds(q * HD, HD)
            high = pl.ds((q + CMP_STRIDE) * HD, HD)
            right.append(jnp.concatenate([ink_ref[low, :], ink_ref[high, :], zero, zero], 1))
            right.append(jnp.concatenate([zero, zero, inv_ref[low, :], inv_ref[high, :]], 1))
        total = total + dot(jnp.concatenate(left, 1), jnp.concatenate(right, 0))
    low_k, high_k = total[:, :128], total[:, 128:256]
    low_v, high_v = total[:, 256:384], total[:, 384:]
    pre_k = low_k + pltpu.roll(high_k, NSUM - 1, 0)
    pre_v = low_v + pltpu.roll(high_v, NSUM - 1, 0)
    summaries = squeeze_out(
        pre_k, pre_v, outk_ref[...], outv_ref[...], cosine, sine
    )
    payload = jnp.concatenate(
        [
            summaries,
            low_k[NSUM - 1 :], low_v[NSUM - 1 :], high_k[:1], high_v[:1],
            code[:1, :128], code[:1, 128:256], code[:1, 256:384], code[:1, 384:],
        ],
        0,
    ).astype(bf16)
    for peer in range(PEERS):
        payload_ref[peer] = payload


def project_kernel(
    rank_ref, tokens_ref, wq_ref, wk_ref, wv_ref, gate_ref, cos_ref, sin_ref, chosen_ref, code_ref,
    query_ref, pair_ref, gates_ref, place_ref, bound_ref,
    weight_ref,
):
    @pl.when(pl.program_id(0) == 0)
    def _():
        weight_ref[:HD] = wk_ref[...]
        weight_ref[HD : 2 * HD] = wv_ref[...]
        weight_ref[2 * HD :] = jnp.concatenate([gate_ref[0], gate_ref[1]], 0)
        rank = rank_ref[0]
        chosen = chosen_ref[...]
        query_block = rank * QB + rows_of(chosen.shape)
        code = code_ref[...]
        code = jnp.concatenate([code, code], 0)
        every = lanes_of((QB, NBLK))
        slot_lane = lanes_of((QB, NSEL))
        slot = jnp.zeros((QB, NSEL), f32)
        for k in range(NSEL):
            found = jnp.where(every == chosen[:, k : k + 1], code, 0.0)
            slot = jnp.where(slot_lane == k, jnp.sum(found, 1, keepdims=True), slot)
        holder = chosen // QB
        place = jnp.where(
            holder == rank, PEERS * CAP + chosen % QB, holder * CAP + slot.astype(jnp.int32)
        )
        place_ref[...] = jnp.where(chosen <= query_block, place, PEERS * CAP)
        order = jnp.where(chosen < query_block, -1.0, jnp.where(chosen > query_block, 1.0, 0.0))
        spread = (lanes_of((NSEL, NSEL * BLK)) // BLK == rows_of((NSEL, NSEL * BLK))).astype(bf16)
        inner = (lanes_of((QB, NSEL * BLK)) % BLK).astype(f32)
        bound_ref[...] = dot(order.astype(bf16), spread) * 64.0 + inner

    tokens = tokens_ref[...]
    cosine = cos_ref[...]
    sine = sin_ref[...]
    lane = lanes_of(cosine.shape)
    both = dot_t(tokens, weight_ref[...])
    pair = both[:, : 2 * HD]
    pair_ref[...] = jnp.where(lane < HD, turned(pair, cosine, sine), pair).astype(bf16)
    gates_ref[...] = jax.nn.sigmoid(both[:, 2 * HD :])
    queries = dot(tokens, wq_ref[...]) * np.float32(HD ** -0.5)
    for side in range(2):
        both = turned(queries[:, 128 * side : 128 * side + 128], cosine, sine)
        for half in range(2):
            head = 2 * side + half
            one = both if half == 0 else pltpu.roll(both, HD, 1)
            one = jnp.where(lane < HD, one, 0.0).astype(bf16)
            for b in range(PART // BLK):
                query_ref[b, head * BLK : (head + 1) * BLK, :] = one[b * BLK : (b + 1) * BLK]


def pick_kernel(rank_ref, arrived_ref, pair_hbm, picked_ref, pair_ref, ids_ref, ids_smem, sems):
    rank = rank_ref[0]
    step = pl.program_id(0)

    @pl.when(step == 0)
    def _():
        load = pltpu.make_async_copy(pair_hbm, pair_ref, sems.at[0])
        load.start()
        flat = arrived_ref[...].reshape(PEERS * ROWS, 128)
        shape = (PEERS, PEERS * ROWS)
        chosen_row = (lanes_of(shape) == rows_of(shape) * ROWS + NSUM + 4 + rank // 8).astype(bf16)
        codes = dot(chosen_row, flat)
        lane = lanes_of((PEERS, 128))
        mine = lane // QB == rank % 8
        inner = (lane % QB).astype(f32)
        ids = jnp.zeros((PEERS, 128), f32)
        for s in range(CAP):
            value = jnp.sum(jnp.where(mine & (codes == float(s)), inner, 0.0), 1, keepdims=True)
            ids = jnp.where(lane == s, value, ids)
        ids_ref[...] = ids.astype(jnp.int32)
        copy = pltpu.make_async_copy(ids_ref, ids_smem, sems.at[1])
        copy.start()
        load.wait()
        copy.wait()

    for peer in range(PICK):
        for s in range(CAP):
            start = pl.multiple_of(ids_smem[step * PICK + peer, s] * BLK, BLK)
            picked_ref[peer, s * BLK : (s + 1) * BLK, :] = pair_ref[pl.ds(start, BLK), :]


def mixed_heads(result, gates, first):
    lane = lanes_of((BLK, 128))
    halves = []
    for pair in range(2):
        gated = []
        for head in (2 * pair, 2 * pair + 1):
            gate = gates[:, first + head : first + head + 1]
            gated.append(result[head * BLK : (head + 1) * BLK] * gate)
        halves.append(jnp.where(lane < HD, pltpu.roll(gated[0], HD, 1), gated[1]))
    return halves


def compressed_kernel(
    rank_ref, arrived_ref, query_ref, gates_ref, outk_ref, outv_ref, cos_ref, sin_ref,
    mixed_ref, key_ref, value_ref,
):
    rank = rank_ref[0]
    flat = arrived_ref[...].reshape(PEERS * ROWS, 128)
    shape = (4 * PEERS, PEERS * ROWS)
    row = rows_of(shape)
    kind = row // PEERS
    source = row % PEERS + kind % 2
    target = source * ROWS + NSUM + jnp.where(kind == 0, 0, jnp.where(kind == 1, 2, jnp.where(kind == 2, 1, 3)))
    edges = dot(((lanes_of(shape) == target) & (source < PEERS)).astype(bf16), flat)
    pre_k = edges[:PEERS] + edges[PEERS : 2 * PEERS]
    pre_v = edges[2 * PEERS : 3 * PEERS] + edges[3 * PEERS :]
    last = squeeze_out(pre_k, pre_v, outk_ref[...], outv_ref[...], cos_ref[...], sin_ref[...])
    is_last = rows_of((NSUM, 128)) == NSUM - 1
    lane = lanes_of((NSUM, 128))
    for peer in range(PEERS):
        chunk = arrived_ref[peer, :NSUM, :].astype(f32)
        chunk = jnp.where(is_last, last[peer : peer + 1], chunk)
        value_ref[peer * NSUM : (peer + 1) * NSUM, :] = jnp.where(lane < HD, 1.0, chunk).astype(bf16)
        key_ref[peer * NSUM : (peer + 1) * NSUM, :] = chunk.astype(bf16)
    columns = lanes_of((HEADS * BLK, PEERS * NSUM))
    inside = lax.broadcasted_iota(jnp.int32, (HEADS * BLK, 1), 0) % BLK

    def some_blocks(step, carry):
        for j in range(AT_ONCE):
            b = step * AT_ONCE + j
            scores = dot_t(query_ref[b], key_ref[...])
            limit = (rank * TOK + b * BLK + inside - (2 * CMP_STRIDE - 1)) >> 4
            scores = jnp.where(columns <= limit, scores, NEG)
            largest = jnp.maximum(jnp.max(scores, 1, keepdims=True), FLOOR)
            weights = jnp.exp(scores - largest).astype(bf16)
            result = dot(weights, value_ref[...])
            result = result / jnp.maximum(pltpu.roll(result, HD, 1), 1.0)
            start = pl.multiple_of(b * BLK, BLK)
            halves = mixed_heads(result, gates_ref[pl.ds(start, BLK), :], 0)
            mixed_ref[pl.ds(start, BLK), :128] = halves[0].astype(bf16)
            mixed_ref[pl.ds(start, BLK), 128:] = halves[1].astype(bf16)
        return carry

    lax.fori_loop(0, QB // AT_ONCE, some_blocks, 0)


def selected_kernel(
    rank_ref, place_ref, fetched_hbm, pair_hbm, query_hbm, gates_hbm, mixed_hbm, bound_hbm,
    out0_ref, out1_ref, out2_ref, out3_ref,
    fetched_ref, pair_ref, query_ref, gates_ref, mixed_ref, bound_ref, key_ref, out_ref, sems,
):
    chip = rank_ref[1]
    copies = [
        (fetched_hbm, fetched_ref),
        (pair_hbm, pair_ref),
        (bound_hbm, bound_ref),
        (query_hbm, query_ref),
        (gates_hbm, gates_ref),
        (mixed_hbm, mixed_ref),
    ]
    copies = [pltpu.make_async_copy(a, b, sems.at[n]) for n, (a, b) in enumerate(copies)]
    for copy in copies:
        copy.start()
    inside = (lax.broadcasted_iota(jnp.int32, (HEADS * BLK, 1), 0) % BLK).astype(f32)
    lane = lanes_of((NSEL * BLK, 128))
    for copy in copies:
        copy.wait()

    def one_chip(d, carry):
        first = ((chip + d) % CHIPS) * PER_CHIP
        for j in range(PER_CHIP):
            b = first + j
            for k in range(NSEL):
                place = place_ref[b, k]
                far_row = pl.multiple_of(jnp.minimum(place, PEERS * CAP - 1) * BLK, BLK)
                near_row = pl.multiple_of(jnp.maximum(place - PEERS * CAP, 0) * BLK, BLK)
                is_near = jnp.full((BLK, 128), place, jnp.int32) >= PEERS * CAP
                key_ref[j, k * BLK : (k + 1) * BLK, :] = jnp.where(
                    is_near, pair_ref[pl.ds(near_row, BLK), :], fetched_ref[pl.ds(far_row, BLK), :]
                )
        for j in range(PER_CHIP):
            b = first + j
            keys = key_ref[j]
            scores = dot_t(query_ref[b], keys)
            scores = jnp.where(bound_ref[pl.ds(b, 1), :] <= inside, scores, NEG)
            largest = jnp.max(scores, 1, keepdims=True)
            weights = jnp.exp(scores - largest).astype(bf16)
            values = jnp.where(lane < HD, jnp.ones_like(keys), keys)
            result = dot(weights, values)
            result = result / pltpu.roll(result, HD, 1)
            start = pl.multiple_of(b * BLK, BLK)
            halves = mixed_heads(result, gates_ref[pl.ds(start, BLK), :], HEADS)
            for side in range(2):
                cols = slice(128 * side, 128 * side + 128)
                out_ref[d, j * BLK : (j + 1) * BLK, cols] = (
                    mixed_ref[pl.ds(start, BLK), cols] + halves[side]
                ).astype(bf16)
        return carry

    lax.fori_loop(0, CHIPS, one_chip, 0)
    for d, ref in enumerate((out0_ref, out1_ref, out2_ref, out3_ref)):
        ref[...] = out_ref[d]


def output_kernel(
    rank_ref, a0_ref, a1_ref, a2_ref, a3_ref, w0_ref, w1_ref, w2_ref, w3_ref,
    mine_ref, other_ref, sum_ref,
):
    core = rank_ref[2]
    total = dot(a0_ref[...], w0_ref[...])
    total = total + dot(a1_ref[...], w1_ref[...])
    total = total + dot(a3_ref[...], w3_ref[...])
    total = total + dot(a2_ref[...], w2_ref[...])
    sum_ref[...] = total
    mine_ref[...] = sum_ref[pl.ds(pl.multiple_of(core * OUT_ROWS, OUT_ROWS), OUT_ROWS), :]
    other = pl.multiple_of((1 - core) * OUT_ROWS, OUT_ROWS)
    other_ref[...] = sum_ref[pl.ds(other, OUT_ROWS), :].astype(bf16)


VMEM = pl.BlockSpec(memory_space=pltpu.VMEM)
SMEM = pl.BlockSpec(memory_space=pltpu.SMEM)
HBM = pl.BlockSpec(memory_space=pltpu.HBM)


def shape_of(shape, dtype):
    return jax.ShapeDtypeStruct(shape, dtype)


def stored(shape, dtype):
    return pltpu.HBM(shape, dtype)


def far(*values):
    return [pltpu.with_memory_space_constraint(value, pltpu.HBM) for value in values]


def limit(mib):
    return pltpu.CompilerParams(vmem_limit_bytes=mib * 1024 * 1024)


def around(value, distance):
    route = [(2 * y + c, 2 * ((y + distance) % CHIPS) + c) for y in range(CHIPS) for c in range(2)]
    return lax.ppermute(value, "tp", route)


def tables(positions):
    angles = positions.astype(f32)[:, None] * jnp.asarray(INVERSE_ROW)
    return jnp.cos(angles), jnp.sin(angles) * jnp.asarray(SIGN_ROW)


def on_device(
    tokens, query_weight, chosen_key_weight, chosen_value_weight, summary_key_weight,
    summary_value_weight, squeeze_key_in, squeeze_key_out, squeeze_value_in, squeeze_value_out,
    gate_weight, output_weight, chosen_blocks,
):
    kv_rank = lax.axis_index("kv")
    tp_rank = lax.axis_index("tp")
    rank = jnp.stack([kv_rank, tp_rank // 2, tp_rank % 2]).astype(jnp.int32)
    chosen = chosen_blocks[0]
    chosen_key_t = chosen_key_weight.T
    chosen_value_t = chosen_value_weight.T
    squeeze_key_t = squeeze_key_out.T
    squeeze_value_t = squeeze_value_out.T
    gate_t = gate_weight.transpose(0, 2, 1)
    turn = jnp.asarray(np.concatenate([INVERSE_ROW, SIGN_ROW], 0))
    payload, code = pl.pallas_call(
        summary_kernel,
        name="summaries",
        out_shape=(shape_of((PEERS, ROWS, 128), bf16), shape_of((8, NBLK), f32)),
        in_specs=[SMEM] + [HBM] * 9,
        out_specs=(VMEM, VMEM),
        scratch_shapes=[
            pltpu.VMEM((TOK, 2048), bf16),
            pltpu.VMEM((2 * HD, 2048), bf16),
            pltpu.VMEM((2048, 128), bf16),
            pltpu.VMEM((2048, 128), bf16),
            pltpu.VMEM((HD, 128), bf16),
            pltpu.VMEM((HD, 128), bf16),
            pltpu.VMEM((2, 128), f32),
            pltpu.VMEM((QB, NSEL), jnp.int32),
            pltpu.VMEM((TOK, 128), f32),
            pltpu.SemaphoreType.DMA((8 + CHUNKS,)),
        ],
        compiler_params=limit(16),
        cost_estimate=pl.CostEstimate(flops=10**9, bytes_accessed=5 * 10**6, transcendentals=0),
    )(
        rank,
        *far(
            tokens, summary_key_weight.T, summary_value_weight.T, squeeze_key_in, squeeze_value_in,
            squeeze_key_t, squeeze_value_t, turn, chosen,
        ),
    )
    weight_1 = around(output_weight, 1)
    weight_3 = around(output_weight, -1)
    arrived = lax.all_to_all(payload, "kv", 0, 0, tiled=True)
    cosine, sine = tables(kv_rank * TOK + jnp.arange(TOK, dtype=jnp.int32))
    queries, pairs, gates, place, bound = pl.pallas_call(
        project_kernel,
        name="projections",
        out_shape=(
            stored((QB, HEADS * BLK, 128), bf16),
            stored((TOK, 128), bf16),
            stored((TOK, 2 * HEADS), f32),
            stored((QB, NSEL), jnp.int32),
            stored((QB, NSEL * BLK), f32),
        ),
        grid=(TOK // PART,),
        in_specs=[
            SMEM,
            pl.BlockSpec((PART, 2048), lambda n: (n, 0)),
            VMEM, VMEM, VMEM, VMEM,
            pl.BlockSpec((PART, 128), lambda n: (n, 0)),
            pl.BlockSpec((PART, 128), lambda n: (n, 0)),
            VMEM, VMEM,
        ],
        out_specs=(
            pl.BlockSpec((PART // BLK, HEADS * BLK, 128), lambda n: (n, 0, 0)),
            pl.BlockSpec((PART, 128), lambda n: (n, 0)),
            pl.BlockSpec((PART, 2 * HEADS), lambda n: (n, 0)),
            VMEM, VMEM,
        ),
        scratch_shapes=[pltpu.VMEM((2 * HD + 2 * HEADS, 2048), bf16)],
        compiler_params=limit(20),
        cost_estimate=pl.CostEstimate(flops=10**10, bytes_accessed=5 * 10**6, transcendentals=0),
    )(
        rank,
        *far(tokens, query_weight, chosen_key_t, chosen_value_t),
        gate_t, cosine, sine, chosen, code,
    )
    picked = pl.pallas_call(
        pick_kernel,
        name="pick",
        out_shape=shape_of((PEERS, CAP * BLK, 128), bf16),
        grid=(PEERS // PICK,),
        in_specs=[SMEM, VMEM, HBM],
        out_specs=pl.BlockSpec((PICK, CAP * BLK, 128), lambda step: (step, 0, 0)),
        scratch_shapes=[
            pltpu.VMEM((TOK, 128), bf16),
            pltpu.VMEM((PEERS, 128), jnp.int32),
            pltpu.SMEM((PEERS, 128), jnp.int32),
            pltpu.SemaphoreType.DMA((2,)),
        ],
        compiler_params=limit(8),
    )(rank, arrived, *far(pairs))
    fetched = lax.all_to_all(picked, "kv", 0, 0, tiled=True)
    last_cos, last_sin = tables(jnp.arange(PEERS, dtype=jnp.int32) * TOK + (TOK + CMP_STRIDE - 1))
    mixed = pl.pallas_call(
        compressed_kernel,
        name="compressed",
        out_shape=stored((TOK, HEADS * HD), bf16),
        in_specs=[SMEM] + [VMEM] * 7,
        out_specs=VMEM,
        scratch_shapes=[
            pltpu.VMEM((PEERS * NSUM, 128), bf16),
            pltpu.VMEM((PEERS * NSUM, 128), bf16),
        ],
        compiler_params=limit(16),
        cost_estimate=pl.CostEstimate(flops=10**10, bytes_accessed=3 * 10**6, transcendentals=0),
    )(rank, arrived, *far(queries, gates), squeeze_key_t, squeeze_value_t, last_cos, last_sin)
    weight_1, mixed = lax.optimization_barrier((weight_1, mixed))
    weight_2 = around(weight_1, 1)

    pieces = pl.pallas_call(
        selected_kernel,
        name="selected",
        out_shape=(shape_of((PER_CHIP * BLK, HEADS * HD), bf16),) * CHIPS,
        in_specs=[SMEM, SMEM] + [HBM] * 6,
        out_specs=(VMEM,) * CHIPS,
        scratch_shapes=[
            pltpu.VMEM((PEERS * CAP * BLK, 128), bf16),
            pltpu.VMEM((TOK, 128), bf16),
            pltpu.VMEM((QB, HEADS * BLK, 128), bf16),
            pltpu.VMEM((TOK, 2 * HEADS), f32),
            pltpu.VMEM((TOK, HEADS * HD), bf16),
            pltpu.VMEM((QB, NSEL * BLK), f32),
            pltpu.VMEM((PER_CHIP, NSEL * BLK, 128), bf16),
            pltpu.VMEM((CHIPS, PER_CHIP * BLK, HEADS * HD), bf16),
            pltpu.SemaphoreType.DMA((6,)),
        ],
        compiler_params=limit(16),
        cost_estimate=pl.CostEstimate(flops=10**9, bytes_accessed=3 * 10**6, transcendentals=0),
    )(
        rank, place,
        *far(fetched.reshape(PEERS * CAP * BLK, 128), pairs, queries, gates, mixed, bound),
    )
    piece_2 = around(pieces[2], 2)
    piece_1 = around(pieces[1], 1)
    piece_3 = around(pieces[3], -1)
    mine, other = pl.pallas_call(
        output_kernel,
        name="output",
        out_shape=(shape_of((OUT_ROWS, 2048), f32), shape_of((OUT_ROWS, 2048), bf16)),
        in_specs=[SMEM] + [VMEM] * 8,
        out_specs=(VMEM, VMEM),
        scratch_shapes=[pltpu.VMEM((2 * OUT_ROWS, 2048), f32)],
        compiler_params=limit(16),
    )(
        rank, pieces[0], piece_1, piece_2, piece_3, output_weight, weight_1, weight_2, weight_3,
    )
    swapped = lax.ppermute(other, "tp", [(i, i ^ 1) for i in range(2 * CHIPS)])
    return (mine + swapped.astype(f32)).astype(bf16)


def solution(mesh):
    return jax.shard_map(
        on_device,
        mesh=mesh,
        in_specs=(
            P("kv", None),
            P(None, "tp"),
            P(None, "tp"),
            P(None, "tp"),
            P(None, "tp"),
            P(None, "tp"),
            P(),
            P(),
            P(),
            P(),
            P(None, None, "tp"),
            P("tp", None),
            P("tp", "kv", None),
        ),
        out_specs=P(("kv", "tp"), None),
        check_vma=False,
    )
```

profile of v0, /device:TPU:1, one launch (start us, length us, event | category | flops | bytes accessed | tf_op | source)
XLA Modules:
  0.0 89.3 jit_solution(7866207240272593603)
XLA Ops:
  0.0 2.1 %collective-permute-start = (bf16[256,2048]{1,0:T(8,128)(2,1)}, bf16[256,2048]{1,0:T(8,128)(2,1)S(1)}, u32[]{:S(2)}, u32[]{:S(2)}) collective-permute-start(bf16[256,2048]{1,0:T(8,128)(2,1)} %w0_ref.1), channel_id=1, source_target_pairs={{0,2},{1,3},{2,4},{3,5},{4,6},{5,7},{6,0},{7,1},{8,10},{9,11},{10,... | collective-permute-start | bytes 3145736 | tf_op jit(solution)/shard_map/ppermute | solution.py:390
  2.1 1.4 %collective-permute-start.5 = (bf16[256,2048]{1,0:T(8,128)(2,1)}, bf16[256,2048]{1,0:T(8,128)(2,1)S(1)}, u32[]{:S(2)}, u32[]{:S(2)}) collective-permute-start(bf16[256,2048]{1,0:T(8,128)(2,1)} %w0_ref.1), channel_id=1, source_target_pairs={{0,6},{1,7},{2,0},{3,1},{4,2},{5,3},{6,4},{7,5},{8,14},{9,15},{10,... | collective-permute-start | bytes 3145736 | tf_op jit(solution)/shard_map/ppermute | solution.py:390
  3.6 0.1 pad_add_fusion.rank_ref
  3.6 4.8 %summaries.1 = (bf16[32,40,128]{2,1,0:T(8,128)(2,1)}, f32[8,512]{1,0:T(8,128)S(1)}) custom-call(s32[3]{0:T(128)S(1)} %pad_add_fusion.rank_ref, bf16[512,2048]{1,0:T(8,128)(2,1)} %tokens_ref.1, bf16[64,2048]{1,0:T(8,128)(2,1)} %bitcast.19, bf16[64,2048]{1,0:T(8,128)(2,1)} %bitcast.20, bf16[2048,128]{1,0:T(8,128)(2,1)} %ink_hbm.1, bf16[2048,128]{1,0:T(8,128)(2,1)} %inv_hbm.1, ...), custom_call_target="tpu_custom_call" | custom-call | flops 1000000000 | bytes 5000000 | tf_op jit(solution)/shard_map/summaries/pallas_call | solution.py:413
  8.4 11.0 %all-to-all-start = ((bf16[32,40,128]{2,1,0:T(8,128)(2,1)}), bf16[32,40,128]{2,1,0:T(8,128)(2,1)S(1)}, u32[]{:S(2)}, u32[]{:S(2)}) async-start(bf16[32,40,128]{2,1,0:T(8,128)(2,1)} %get-tuple-element.22), calls=%async_computation | async-start | bytes 655360 | tf_op jit(solution)/shard_map/all_to_all | solution.py:442
  19.5 0.0 copy-done.6
  19.5 0.0 copy-done.7
  19.5 1.0 %fusion = (f32[512,128]{1,0:T(8,128)S(1)}, f32[512,128]{1,0:T(8,128)S(1)}) fusion(f32[128]{0:T(128)S(1)} %copy-done.6, f32[128]{0:T(128)S(1)} %copy-done.7, f32[512]{0:T(512)S(1)} %add_convert_fusion.1), kind=kLoop, calls=%fused_computation.3 | loop fusion | flops 131072 | bytes 527360 | tf_op jit(solution)/shard_map/mul | solution.py:395
  20.6 6.2 %projections.1 = (bf16[16,128,128]{2,1,0:T(8,128)(2,1)}, bf16[512,128]{1,0:T(8,128)(2,1)}, f32[512,8]{1,0:T(8,128)}, s32[16,16]{1,0:T(8,128)}, f32[16,512]{1,0:T(8,128)}) custom-call(s32[3]{0:T(128)S(1)} %pad_add_fusion.rank_ref, bf16[512,2048]{1,0:T(8,128)(2,1)} %tokens_ref.1, bf16[2048,256]{1,0:T(8,128)(2,1)} %wq_ref.1, bf16[64,2048]{1,0:T(8,128)(2,1)} %bitcast.21, ...), custom_call_target="tpu_custom_call" | custom-call | flops 10000000000 | bytes 5000000 | tf_op jit(solution)/shard_map/projections/pallas_call | solution.py:444
  26.7 0.0 copy-start.2
  26.7 4.8 %all-to-all-done.arrived_ref = bf16[32,40,128]{2,1,0:T(8,128)(2,1)S(1)} async-done(((bf16[32,40,128]{2,1,0:T(8,128)(2,1)}), bf16[32,40,128]{2,1,0:T(8,128)(2,1)S(1)}, u32[]{:S(2)}, u32[]{:S(2)}) %all-to-all-start) | async-done | bytes 327712 | tf_op jit(solution)/shard_map/all_to_all | solution.py:442
  31.6 3.3 %pick.1 = bf16[32,128,128]{2,1,0:T(8,128)(2,1)} custom-call(s32[3]{0:T(128)S(1)} %pad_add_fusion.rank_ref, bf16[32,40,128]{2,1,0:T(8,128)(2,1)S(1)} %all-to-all-done.arrived_ref, bf16[512,128]{1,0:T(8,128)(2,1)} %get-tuple-element.23.pair_hbm), custom_call_target="tpu_custom_call" | custom-call | tf_op jit(solution)/shard_map/pick/pallas_call | solution.py:477
  34.9 5.3 %all-to-all-start.1 = ((bf16[32,128,128]{2,1,0:T(8,128)(2,1)}), bf16[32,128,128]{2,1,0:T(8,128)(2,1)}, u32[]{:S(2)}, u32[]{:S(2)}) async-start(bf16[32,128,128]{2,1,0:T(8,128)(2,1)} %pick.1), calls=%async_computation.1 | async-start | bytes 2097152 | tf_op jit(solution)/shard_map/all_to_all | solution.py:492
  40.2 0.1 fusion.1
  40.4 10.3 %compressed.1.mixed_hbm = bf16[512,256]{1,0:T(8,128)(2,1)} custom-call(s32[3]{0:T(128)S(1)} %pad_add_fusion.rank_ref, bf16[32,40,128]{2,1,0:T(8,128)(2,1)S(1)} %all-to-all-done.arrived_ref, bf16[16,128,128]{2,1,0:T(8,128)(2,1)} %get-tuple-element.24.query_ref.query_hbm, f32[512,8]{1,0:T(8,128)} %get-tuple-element.25.gates_ref.gates_hbm, ...), custom_call_target="tpu_custom_call" | custom-call | flops 10000000000 | bytes 3000000 | tf_op jit(solution)/shard_map/compressed/pallas_call | solution.py:494
  50.7 0.0 collective-permute-done.w1_ref
  50.7 0.0 collective-permute-start.4
  50.8 14.7 %all-to-all-done.1 = bf16[32,128,128]{2,1,0:T(8,128)(2,1)} async-done(((bf16[32,128,128]{2,1,0:T(8,128)(2,1)}), bf16[32,128,128]{2,1,0:T(8,128)(2,1)}, u32[]{:S(2)}, u32[]{:S(2)}) %all-to-all-start.1) | async-done | bytes 1048608 | tf_op jit(solution)/shard_map/all_to_all | solution.py:492
  65.4 8.5 %selected.1 = (bf16[128,256]{1,0:T(8,128)(2,1)S(1)}, bf16[128,256]{1,0:T(8,128)(2,1)S(1)}, bf16[128,256]{1,0:T(8,128)(2,1)S(1)}, bf16[128,256]{1,0:T(8,128)(2,1)S(1)}) custom-call(s32[3]{0:T(128)S(1)} %pad_add_fusion.rank_ref, s32[16,16]{1,0:T(8,128)S(1)} %copy-done.5, bf16[4096,128]{1,0:T(8,128)(2,1)} %bitcast.11.fetched_hbm, ...), custom_call_target="tpu_custom_call" | custom-call | flops 1000000000 | bytes 3000000 | tf_op jit(solution)/shard_map/selected/pallas_call | solution.py:510
  74.0 0.1 collective-permute-start.1
  74.1 2.6 %collective-permute-start.2 = (bf16[128,256]{1,0:T(8,128)(2,1)S(1)}, bf16[128,256]{1,0:T(8,128)(2,1)S(1)}, u32[]{:S(2)}, u32[]{:S(2)}) collective-permute-start(bf16[128,256]{1,0:T(8,128)(2,1)S(1)} %get-tuple-element.30), channel_id=1, source_target_pairs={{0,4},{1,5},{2,6},{3,7},{4,0},{5,1},{6,2},{7,3},{8,12},{9,13},{10,... | collective-permute-start | bytes 196616 | tf_op jit(solution)/shard_map/ppermute | solution.py:390
  76.7 1.1 %collective-permute-start.3 = (bf16[128,256]{1,0:T(8,128)(2,1)S(1)}, bf16[128,256]{1,0:T(8,128)(2,1)S(1)}, u32[]{:S(2)}, u32[]{:S(2)}) collective-permute-start(bf16[128,256]{1,0:T(8,128)(2,1)S(1)} %get-tuple-element.31), channel_id=1, source_target_pairs={{0,6},{1,7},{2,0},{3,1},{4,2},{5,3},{6,4},{7,5},{8,14},{9,15},{10,... | collective-permute-start | bytes 196616 | tf_op jit(solution)/shard_map/ppermute | solution.py:390
  77.8 0.0 collective-permute-done.5.w3_ref
  77.8 0.0 collective-permute-done.4.w2_ref
  77.8 0.6 collective-permute-done.1.a1_ref
  78.4 0.7 collective-permute-done.2.a2_ref
  79.1 0.7 collective-permute-done.3.a3_ref
  79.8 0.0 copy-done
  79.8 2.0 %output.1 = (f32[64,2048]{1,0:T(8,128)S(1)}, bf16[64,2048]{1,0:T(8,128)(2,1)S(1)}) custom-call(s32[3]{0:T(128)S(1)} %pad_add_fusion.rank_ref, bf16[128,256]{1,0:T(8,128)(2,1)S(1)} %get-tuple-element.28.a0_ref, bf16[128,256]{1,0:T(8,128)(2,1)S(1)} %collective-permute-done.1.a1_ref, bf16[128,256]{1,0:T(8,128)(2,1)S(1)} %collective-permute-done.2.a2_ref, ...), custom_call_target="tpu_custom_call" | custom-call | tf_op jit(solution)/shard_map/output/pallas_call | solution.py:536
  81.8 5.6 %collective-permute-start.6 = (bf16[64,2048]{1,0:T(8,128)(2,1)S(1)}, bf16[64,2048]{1,0:T(8,128)(2,1)S(1)}, u32[]{:S(2)}, u32[]{:S(2)}) collective-permute-start(bf16[64,2048]{1,0:T(8,128)(2,1)S(1)} %get-tuple-element.34), channel_id=1, source_target_pairs={{0,1},{1,0},{2,3},{3,2},{4,5},{5,4},{6,7},{7,6},{8,9},{9,8},{10,11... | collective-permute-start | bytes 786440 | tf_op jit(solution)/shard_map/ppermute | solution.py:547
  87.4 1.2 %collective-permute-done.6 = bf16[64,2048]{1,0:T(8,128)(2,1)S(1)} collective-permute-done((bf16[64,2048]{1,0:T(8,128)(2,1)S(1)}, bf16[64,2048]{1,0:T(8,128)(2,1)S(1)}, u32[]{:S(2)}, u32[]{:S(2)}) %collective-permute-start.6) | collective-permute-done | bytes 262176 | tf_op jit(solution)/shard_map/ppermute | solution.py:547
  88.6 0.8 add_convert_fusion
  (14 shorter events, 0.0 us)
Async XLA Ops:
  0.0 50.7 %collective-permute-start = (bf16[256,2048]{1,0:T(8,128)(2,1)}, bf16[256,2048]{1,0:T(8,128)(2,1)S(1)}, u32[]{:S(2)}, u32[]{:S(2)}) collective-permute-start(bf16[256,2048]{1,0:T(8,128)(2,1)} %w0_ref.1), channel_id=1, source_target_pairs={{0,2},{1,3},{2,4},{3,5},{4,6},{5,7},{6,0},{7,1},{8,10},{9,11},{10,... | collective-permute-start | bytes 3145736 | tf_op jit(solution)/shard_map/ppermute | solution.py:390
  2.1 75.6 %collective-permute-start.5 = (bf16[256,2048]{1,0:T(8,128)(2,1)}, bf16[256,2048]{1,0:T(8,128)(2,1)S(1)}, u32[]{:S(2)}, u32[]{:S(2)}) collective-permute-start(bf16[256,2048]{1,0:T(8,128)(2,1)} %w0_ref.1), channel_id=1, source_target_pairs={{0,6},{1,7},{2,0},{3,1},{4,2},{5,3},{6,4},{7,5},{8,14},{9,15},{10,... | collective-permute-start | bytes 3145736 | tf_op jit(solution)/shard_map/ppermute | solution.py:390
  3.6 15.9 %copy-start.6 = (f32[128]{0:T(128)S(1)}, f32[128]{0:T(128)}, u32[]{:S(2)}) copy-start(f32[128]{0:T(128)} %constant.50) | copy-start | bytes 1540
  3.6 15.9 %copy-start.7 = (f32[128]{0:T(128)S(1)}, f32[128]{0:T(128)}, u32[]{:S(2)}) copy-start(f32[128]{0:T(128)} %constant.49) | copy-start | bytes 1540
  3.6 16.9 %copy-start.3 = (s32[1,16,16]{2,1,0:T(8,128)S(1)}, s32[1,16,16]{2,1,0:T(8,128)}, u32[]{:S(2)}) copy-start(s32[1,16,16]{2,1,0:T(8,128)} %param.28) | copy-start | bytes 3076
  3.6 16.9 %copy-start.4 = (bf16[2,2048,4]{1,2,0:T(4,128)(2,1)S(1)}, bf16[2,2048,4]{1,2,0:T(4,128)(2,1)}, u32[]{:S(2)}) copy-start(bf16[2,2048,4]{1,2,0:T(4,128)(2,1)} %param.26) | copy-start | bytes 98308
  8.4 23.2 %all-to-all-start = ((bf16[32,40,128]{2,1,0:T(8,128)(2,1)}), bf16[32,40,128]{2,1,0:T(8,128)(2,1)S(1)}, u32[]{:S(2)}, u32[]{:S(2)}) async-start(bf16[32,40,128]{2,1,0:T(8,128)(2,1)} %get-tuple-element.22), calls=%async_computation | async-start | bytes 655360 | tf_op jit(solution)/shard_map/all_to_all | solution.py:442
  26.7 13.6 %copy-start.1 = (bf16[128,64]{0,1:T(8,128)(2,1)S(1)}, bf16[128,64]{0,1:T(8,128)(2,1)}, u32[]{:S(2)}) copy-start(bf16[128,64]{0,1:T(8,128)(2,1)} %param.23) | copy-start | bytes 49156
  26.7 13.6 %copy-start.2 = (bf16[128,64]{0,1:T(8,128)(2,1)S(1)}, bf16[128,64]{0,1:T(8,128)(2,1)}, u32[]{:S(2)}) copy-start(bf16[128,64]{0,1:T(8,128)(2,1)} %param.25) | copy-start | bytes 49156
  34.9 30.6 %all-to-all-start.1 = ((bf16[32,128,128]{2,1,0:T(8,128)(2,1)}), bf16[32,128,128]{2,1,0:T(8,128)(2,1)}, u32[]{:S(2)}, u32[]{:S(2)}) async-start(bf16[32,128,128]{2,1,0:T(8,128)(2,1)} %pick.1), calls=%async_computation.1 | async-start | bytes 2097152 | tf_op jit(solution)/shard_map/all_to_all | solution.py:492
  40.4 25.1 %copy-start.5 = (s32[16,16]{1,0:T(8,128)S(1)}, s32[16,16]{1,0:T(8,128)}, u32[]{:S(2)}) copy-start(s32[16,16]{1,0:T(8,128)} %get-tuple-element.21.place_ref) | copy-start | bytes 3076
  50.7 29.1 %copy-start = (bf16[256,2048]{1,0:T(8,128)(2,1)S(1)}, bf16[256,2048]{1,0:T(8,128)(2,1)}, u32[]{:S(2)}) copy-start(bf16[256,2048]{1,0:T(8,128)(2,1)} %w0_ref.1) | copy-start | bytes 3145732
  50.7 27.0 %collective-permute-start.4 = (bf16[256,2048]{1,0:T(8,128)(2,1)S(1)}, bf16[256,2048]{1,0:T(8,128)(2,1)}, u32[]{:S(2)}, u32[]{:S(2)}) collective-permute-start(bf16[256,2048]{1,0:T(8,128)(2,1)S(1)} %collective-permute-done.w1_ref), channel_id=1, source_target_pairs={{0,2},{1,3},{2,4},{3,5},{4,6},{5,7},{6,0},{7,1},{8,10},{9,11},{10,... | collective-permute-start | bytes 3145736 | tf_op jit(solution)/shard_map/ppermute | solution.py:390
  74.0 4.4 %collective-permute-start.1 = (bf16[128,256]{1,0:T(8,128)(2,1)S(1)}, bf16[128,256]{1,0:T(8,128)(2,1)S(1)}, u32[]{:S(2)}, u32[]{:S(2)}) collective-permute-start(bf16[128,256]{1,0:T(8,128)(2,1)S(1)} %get-tuple-element.29), channel_id=1, source_target_pairs={{0,2},{1,3},{2,4},{3,5},{4,6},{5,7},{6,0},{7,1},{8,10},{9,11},{10,... | collective-permute-start | bytes 196616 | tf_op jit(solution)/shard_map/ppermute | solution.py:390
  74.1 5.0 %collective-permute-start.2 = (bf16[128,256]{1,0:T(8,128)(2,1)S(1)}, bf16[128,256]{1,0:T(8,128)(2,1)S(1)}, u32[]{:S(2)}, u32[]{:S(2)}) collective-permute-start(bf16[128,256]{1,0:T(8,128)(2,1)S(1)} %get-tuple-element.30), channel_id=1, source_target_pairs={{0,4},{1,5},{2,6},{3,7},{4,0},{5,1},{6,2},{7,3},{8,12},{9,13},{10,... | collective-permute-start | bytes 196616 | tf_op jit(solution)/shard_map/ppermute | solution.py:390
  76.7 3.1 %collective-permute-start.3 = (bf16[128,256]{1,0:T(8,128)(2,1)S(1)}, bf16[128,256]{1,0:T(8,128)(2,1)S(1)}, u32[]{:S(2)}, u32[]{:S(2)}) collective-permute-start(bf16[128,256]{1,0:T(8,128)(2,1)S(1)} %get-tuple-element.31), channel_id=1, source_target_pairs={{0,6},{1,7},{2,0},{3,1},{4,2},{5,3},{6,4},{7,5},{8,14},{9,15},{10,... | collective-permute-start | bytes 196616 | tf_op jit(solution)/shard_map/ppermute | solution.py:390
  81.8 6.7 %collective-permute-start.6 = (bf16[64,2048]{1,0:T(8,128)(2,1)S(1)}, bf16[64,2048]{1,0:T(8,128)(2,1)S(1)}, u32[]{:S(2)}, u32[]{:S(2)}) collective-permute-start(bf16[64,2048]{1,0:T(8,128)(2,1)S(1)} %get-tuple-element.34), channel_id=1, source_target_pairs={{0,1},{1,0},{2,3},{3,2},{4,5},{5,4},{6,7},{7,6},{8,9},{9,8},{10,11... | collective-permute-start | bytes 786440 | tf_op jit(solution)/shard_map/ppermute | solution.py:547
where the time goes:
time: 89.8 us; the launch traced here: 89.3 us
  Pallas kernels  35.1 us (39%)
  starting transfers between devices  29.3 us (33%)
  waiting for transfers between devices  22.7 us (25%)
  other arithmetic  1.97 us (2%)
    all_to_all x1, waiting for transfers between devices, on_device(): fetched = lax.all_to_all(picked, 'kv', 0, 0, tiled=True)  14.7 us
    all_to_all x1, starting transfers between devices, on_device(): arrived = lax.all_to_all(payload, 'kv', 0, 0, tiled=True)  11 us
    pallas_call x1, Pallas kernels, on_device(): pl.pallas_call(compressed_kernel, name='compressed', out_shape=stored((TO...  10.3 us
    pallas_call x1, Pallas kernels, on_device(): pl.pallas_call(selected_kernel, name='selected', out_shape=(shape_of((PER...  8.54 us
    ppermute x6, starting transfers between devices, around(): return lax.ppermute(value, 'tp', route)  7.37 us
    pallas_call x1, Pallas kernels, on_device(): pl.pallas_call(project_kernel, name='projections', out_shape=(stored((QB,...  6.17 us
    ppermute x1, starting transfers between devices, on_device(): swapped = lax.ppermute(other, 'tp', [(i, i ^ 1) for i in range(2 * CHIPS)])  5.57 us
    all_to_all x1, starting transfers between devices, on_device(): fetched = lax.all_to_all(picked, 'kv', 0, 0, tiled=True)  5.34 us
  transfers between devices with their start and end apart: 9, of which 6 were waited for; matrix products, arithmetic and copies ran while one was open for 1% of the time, Pallas kernels for 37%

commit v1 on v0

--- a/solution.py
+++ b/solution.py
@@ -23,12 +23,15 @@
 HEADS = 4
 NBLK = PEERS * QB
 UNUSED = 99.0
-AT_ONCE = 4
+COMPRESSED = 4
 CHIPS = 4
 PER_CHIP = QB // CHIPS
 CHUNKS = 2
-PICK = 8
-PART = 128
+PICK = 16
+PART = 256
+GATHERED = 8
+WEIGHED = 4
+MIXED = 8
 OUT_ROWS = TOK // 8
 
 INVERSE = (ROTARY_BASE ** (-np.arange(HD // 2, dtype=np.float64) / (HD // 2))).astype(np.float32)
@@ -59,6 +62,11 @@
     lane = lanes_of(x.shape)
     swapped = jnp.where(lane % HD < HD // 2, pltpu.roll(x, 128 - HD // 2, 1), pltpu.roll(x, HD // 2, 1))
     return x * cosine + swapped * sine
+
+
+def turns(positions, turn_ref):
+    angles = positions.astype(f32) * turn_ref[:1]
+    return jnp.cos(angles), jnp.sin(angles) * turn_ref[1:]
 
 
 def gelu(x):
@@ -76,11 +84,11 @@
 
 
 def summary_kernel(
-    rank_ref, tokens_hbm, wk_hbm, wv_hbm, ink_hbm, inv_hbm, outk_hbm, outv_hbm, turn_hbm, chosen_hbm,
+    tokens_hbm, wk_hbm, wv_hbm, ink_hbm, inv_hbm, outk_hbm, outv_hbm, turn_hbm, chosen_hbm,
     payload_ref, code_ref,
     tokens_ref, weight_ref, ink_ref, inv_ref, outk_ref, outv_ref, turn_ref, chosen_ref, raw_ref, sems,
 ):
-    rank = rank_ref[0]
+    rank = lax.axis_index("kv")
     part = TOK // CHUNKS
     copies = [
         (chosen_hbm, chosen_ref),
@@ -120,9 +128,7 @@
     for copy in copies[3 + CHUNKS :]:
         copy.wait()
     ends = (rank * NSUM + rows_of((NSUM, 128))) * CMP_STRIDE + 2 * CMP_STRIDE - 1
-    angles = ends.astype(f32) * turn_ref[:1]
-    cosine = jnp.cos(angles)
-    sine = jnp.sin(angles) * turn_ref[1:]
+    cosine, sine = turns(ends, turn_ref)
     zero = jnp.zeros((HD, 128), bf16)
     total = jnp.zeros((NSUM, 512), f32)
     for p in range(0, CMP_STRIDE, 2):
@@ -154,17 +160,31 @@
         payload_ref[peer] = payload
 
 
-def project_kernel(
-    rank_ref, tokens_ref, wq_ref, wk_ref, wv_ref, gate_ref, cos_ref, sin_ref, chosen_ref, code_ref,
-    query_ref, pair_ref, gates_ref, place_ref, bound_ref,
-    weight_ref,
+def pair_kernel(
+    tokens_ref, wk_ref, wv_ref, gate_ref, cos_ref, sin_ref, pair_ref, gates_ref, weight_ref
 ):
     @pl.when(pl.program_id(0) == 0)
     def _():
         weight_ref[:HD] = wk_ref[...]
         weight_ref[HD : 2 * HD] = wv_ref[...]
         weight_ref[2 * HD :] = jnp.concatenate([gate_ref[0], gate_ref[1]], 0)
-        rank = rank_ref[0]
+
+    both = dot_t(tokens_ref[...], weight_ref[...])
+    pair = both[:, : 2 * HD]
+    lane = lanes_of(pair.shape)
+    pair_ref[...] = jnp.where(
+        lane < HD, turned(pair, cos_ref[...], sin_ref[...]), pair
+    ).astype(bf16)
+    gates_ref[...] = jax.nn.sigmoid(both[:, 2 * HD :])
+
+
+def query_kernel(
+    tokens_ref, wq_ref, cos_ref, sin_ref, chosen_ref, code_ref,
+    query_ref, place_ref, bound_ref,
+):
+    @pl.when(pl.program_id(0) == 0)
+    def _():
+        rank = lax.axis_index("kv")
         chosen = chosen_ref[...]
         query_block = rank * QB + rows_of(chosen.shape)
         code = code_ref[...]
@@ -185,15 +205,10 @@
         inner = (lanes_of((QB, NSEL * BLK)) % BLK).astype(f32)
         bound_ref[...] = dot(order.astype(bf16), spread) * 64.0 + inner
 
-    tokens = tokens_ref[...]
     cosine = cos_ref[...]
     sine = sin_ref[...]
     lane = lanes_of(cosine.shape)
-    both = dot_t(tokens, weight_ref[...])
-    pair = both[:, : 2 * HD]
-    pair_ref[...] = jnp.where(lane < HD, turned(pair, cosine, sine), pair).astype(bf16)
-    gates_ref[...] = jax.nn.sigmoid(both[:, 2 * HD :])
-    queries = dot(tokens, wq_ref[...]) * np.float32(HD ** -0.5)
+    queries = dot(tokens_ref[...], wq_ref[...]) * np.float32(HD ** -0.5)
     for side in range(2):
         both = turned(queries[:, 128 * side : 128 * side + 128], cosine, sine)
         for half in range(2):
@@ -204,8 +219,8 @@
                 query_ref[b, head * BLK : (head + 1) * BLK, :] = one[b * BLK : (b + 1) * BLK]
 
 
-def pick_kernel(rank_ref, arrived_ref, pair_hbm, picked_ref, pair_ref, ids_ref, ids_smem, sems):
-    rank = rank_ref[0]
+def pick_kernel(arrived_ref, pair_hbm, picked_ref, pair_ref, ids_ref, ids_smem, sems):
+    rank = lax.axis_index("kv")
     step = pl.program_id(0)
 
     @pl.when(step == 0)
@@ -248,10 +263,10 @@
 
 
 def compressed_kernel(
-    rank_ref, arrived_ref, query_ref, gates_ref, outk_ref, outv_ref, cos_ref, sin_ref,
-    mixed_ref, key_ref, value_ref,
+    arrived_ref, query_ref, gates_ref, outk_ref, outv_ref, turn_ref, mixed_ref,
+    key_ref, value_ref, score_ref, weight_ref,
 ):
-    rank = rank_ref[0]
+    rank = lax.axis_index("kv")
     flat = arrived_ref[...].reshape(PEERS * ROWS, 128)
     shape = (4 * PEERS, PEERS * ROWS)
     row = rows_of(shape)
@@ -261,7 +276,8 @@
     edges = dot(((lanes_of(shape) == target) & (source < PEERS)).astype(bf16), flat)
     pre_k = edges[:PEERS] + edges[PEERS : 2 * PEERS]
     pre_v = edges[2 * PEERS : 3 * PEERS] + edges[3 * PEERS :]
-    last = squeeze_out(pre_k, pre_v, outk_ref[...], outv_ref[...], cos_ref[...], sin_ref[...])
+    ends = rows_of((PEERS, 128)) * TOK + TOK + CMP_STRIDE - 1
+    last = squeeze_out(pre_k, pre_v, outk_ref[...], outv_ref[...], *turns(ends, turn_ref))
     is_last = rows_of((NSUM, 128)) == NSUM - 1
     lane = lanes_of((NSUM, 128))
     for peer in range(PEERS):
@@ -269,39 +285,55 @@
         chunk = jnp.where(is_last, last[peer : peer + 1], chunk)
         value_ref[peer * NSUM : (peer + 1) * NSUM, :] = jnp.where(lane < HD, 1.0, chunk).astype(bf16)
         key_ref[peer * NSUM : (peer + 1) * NSUM, :] = chunk.astype(bf16)
+    group = COMPRESSED * HEADS * BLK
     columns = lanes_of((HEADS * BLK, PEERS * NSUM))
     inside = lax.broadcasted_iota(jnp.int32, (HEADS * BLK, 1), 0) % BLK
 
-    def some_blocks(step, carry):
-        for j in range(AT_ONCE):
-            b = step * AT_ONCE + j
-            scores = dot_t(query_ref[b], key_ref[...])
+    def score(step, carry):
+        rows = query_ref[pl.ds(step * COMPRESSED, COMPRESSED)].reshape(group, 128)
+        score_ref[pl.ds(pl.multiple_of(step * group, group), group), :] = dot_t(rows, key_ref[...])
+        return carry
+
+    def weigh(step, carry):
+        for j in range(COMPRESSED):
+            b = step * COMPRESSED + j
+            rows = pl.ds(pl.multiple_of(b * HEADS * BLK, HEADS * BLK), HEADS * BLK)
             limit = (rank * TOK + b * BLK + inside - (2 * CMP_STRIDE - 1)) >> 4
-            scores = jnp.where(columns <= limit, scores, NEG)
+            scores = jnp.where(columns <= limit, score_ref[rows, :], NEG)
             largest = jnp.maximum(jnp.max(scores, 1, keepdims=True), FLOOR)
-            weights = jnp.exp(scores - largest).astype(bf16)
-            result = dot(weights, value_ref[...])
-            result = result / jnp.maximum(pltpu.roll(result, HD, 1), 1.0)
-            start = pl.multiple_of(b * BLK, BLK)
-            halves = mixed_heads(result, gates_ref[pl.ds(start, BLK), :], 0)
+            weight_ref[rows, :] = jnp.exp(scores - largest).astype(bf16)
+        return carry
+
+    def mix(step, carry):
+        rows = pl.ds(pl.multiple_of(step * group, group), group)
+        result = dot(weight_ref[rows, :], value_ref[...])
+        result = result / jnp.maximum(pltpu.roll(result, HD, 1), 1.0)
+        for j in range(COMPRESSED):
+            start = pl.multiple_of((step * COMPRESSED + j) * BLK, BLK)
+            one = result[j * HEADS * BLK : (j + 1) * HEADS * BLK]
+            halves = mixed_heads(one, gates_ref[pl.ds(start, BLK), :], 0)
             mixed_ref[pl.ds(start, BLK), :128] = halves[0].astype(bf16)
             mixed_ref[pl.ds(start, BLK), 128:] = halves[1].astype(bf16)
         return carry
 
-    lax.fori_loop(0, QB // AT_ONCE, some_blocks, 0)
+    lax.fori_loop(0, QB // COMPRESSED, score, 0)
+    lax.fori_loop(0, QB // COMPRESSED, weigh, 0)
+    lax.fori_loop(0, QB // COMPRESSED, mix, 0)
 
 
 def selected_kernel(
-    rank_ref, place_ref, fetched_hbm, pair_hbm, query_hbm, gates_hbm, mixed_hbm, bound_hbm,
+    place_hbm, fetched_hbm, pair_hbm, query_hbm, bound_hbm, gates_hbm, mixed_hbm,
     out0_ref, out1_ref, out2_ref, out3_ref,
-    fetched_ref, pair_ref, query_ref, gates_ref, mixed_ref, bound_ref, key_ref, out_ref, sems,
+    place_ref, fetched_ref, pair_ref, query_ref, bound_ref, gates_ref, mixed_ref,
+    key_ref, score_ref, weight_ref, out_ref, sems,
 ):
-    chip = rank_ref[1]
+    chip = lax.axis_index("tp") // 2
     copies = [
+        (place_hbm, place_ref),
         (fetched_hbm, fetched_ref),
         (pair_hbm, pair_ref),
+        (query_hbm, query_ref),
         (bound_hbm, bound_ref),
-        (query_hbm, query_ref),
         (gates_hbm, gates_ref),
         (mixed_hbm, mixed_ref),
     ]
@@ -310,54 +342,69 @@
         copy.start()
     inside = (lax.broadcasted_iota(jnp.int32, (HEADS * BLK, 1), 0) % BLK).astype(f32)
     lane = lanes_of((NSEL * BLK, 128))
-    for copy in copies:
-        copy.wait()
-
-    def one_chip(d, carry):
-        first = ((chip + d) % CHIPS) * PER_CHIP
-        for j in range(PER_CHIP):
-            b = first + j
+
+    def score(step, carry):
+        for j in range(GATHERED):
+            b = step * GATHERED + j
             for k in range(NSEL):
                 place = place_ref[b, k]
                 far_row = pl.multiple_of(jnp.minimum(place, PEERS * CAP - 1) * BLK, BLK)
                 near_row = pl.multiple_of(jnp.maximum(place - PEERS * CAP, 0) * BLK, BLK)
                 is_near = jnp.full((BLK, 128), place, jnp.int32) >= PEERS * CAP
-                key_ref[j, k * BLK : (k + 1) * BLK, :] = jnp.where(
+                key_ref[b, k * BLK : (k + 1) * BLK, :] = jnp.where(
                     is_near, pair_ref[pl.ds(near_row, BLK), :], fetched_ref[pl.ds(far_row, BLK), :]
                 )
-        for j in range(PER_CHIP):
-            b = first + j
-            keys = key_ref[j]
-            scores = dot_t(query_ref[b], keys)
-            scores = jnp.where(bound_ref[pl.ds(b, 1), :] <= inside, scores, NEG)
+            score_ref[b] = dot_t(query_ref[b], key_ref[b])
+        return carry
+
+    def weigh(step, carry):
+        for j in range(WEIGHED):
+            b = step * WEIGHED + j
+            scores = jnp.where(bound_ref[pl.ds(b, 1), :] <= inside, score_ref[b], NEG)
             largest = jnp.max(scores, 1, keepdims=True)
-            weights = jnp.exp(scores - largest).astype(bf16)
+            weight_ref[b] = jnp.exp(scores - largest).astype(bf16)
+        return carry
+
+    def mix(step, carry):
+        for j in range(MIXED):
+            b = step * MIXED + j
+            keys = key_ref[b]
             values = jnp.where(lane < HD, jnp.ones_like(keys), keys)
-            result = dot(weights, values)
+            result = dot(weight_ref[b], values)
             result = result / pltpu.roll(result, HD, 1)
             start = pl.multiple_of(b * BLK, BLK)
             halves = mixed_heads(result, gates_ref[pl.ds(start, BLK), :], HEADS)
+            row = pl.multiple_of((b % PER_CHIP) * BLK, BLK)
             for side in range(2):
                 cols = slice(128 * side, 128 * side + 128)
-                out_ref[d, j * BLK : (j + 1) * BLK, cols] = (
+                out_ref[(b // PER_CHIP - chip + CHIPS) % CHIPS, pl.ds(row, BLK), cols] = (
                     mixed_ref[pl.ds(start, BLK), cols] + halves[side]
                 ).astype(bf16)
         return carry
 
-    lax.fori_loop(0, CHIPS, one_chip, 0)
+    for copy in copies[:4]:
+        copy.wait()
+    lax.fori_loop(0, QB // GATHERED, score, 0)
+    copies[4].wait()
+    lax.fori_loop(0, QB // WEIGHED, weigh, 0)
+    copies[5].wait()
+    copies[6].wait()
+    lax.fori_loop(0, QB // MIXED, mix, 0)
     for d, ref in enumerate((out0_ref, out1_ref, out2_ref, out3_ref)):
         ref[...] = out_ref[d]
 
 
 def output_kernel(
-    rank_ref, a0_ref, a1_ref, a2_ref, a3_ref, w0_ref, w1_ref, w2_ref, w3_ref,
+    a0_ref, a1_ref, a2_ref, a3_ref, w0_ref, w1_ref, w2a_ref, w2b_ref, w3_ref,
     mine_ref, other_ref, sum_ref,
 ):
-    core = rank_ref[2]
+    core = lax.axis_index("tp") % 2
     total = dot(a0_ref[...], w0_ref[...])
     total = total + dot(a1_ref[...], w1_ref[...])
     total = total + dot(a3_ref[...], w3_ref[...])
-    total = total + dot(a2_ref[...], w2_ref[...])
+    half = HEADS * HD // 2
+    total = total + dot(a2_ref[:, :half], w2a_ref[...])
+    total = total + dot(a2_ref[:, half:], w2b_ref[...])
     sum_ref[...] = total
     mine_ref[...] = sum_ref[pl.ds(pl.multiple_of(core * OUT_ROWS, OUT_ROWS), OUT_ROWS), :]
     other = pl.multiple_of((1 - core) * OUT_ROWS, OUT_ROWS)
@@ -401,8 +448,6 @@
     gate_weight, output_weight, chosen_blocks,
 ):
     kv_rank = lax.axis_index("kv")
-    tp_rank = lax.axis_index("tp")
-    rank = jnp.stack([kv_rank, tp_rank // 2, tp_rank % 2]).astype(jnp.int32)
     chosen = chosen_blocks[0]
     chosen_key_t = chosen_key_weight.T
     chosen_value_t = chosen_value_weight.T
@@ -413,8 +458,8 @@
     payload, code = pl.pallas_call(
         summary_kernel,
         name="summaries",
-        out_shape=(shape_of((PEERS, ROWS, 128), bf16), shape_of((8, NBLK), f32)),
-        in_specs=[SMEM] + [HBM] * 9,
+        out_shape=(shape_of((PEERS, ROWS, 128), bf16), stored((8, NBLK), f32)),
+        in_specs=[HBM] * 9,
         out_specs=(VMEM, VMEM),
         scratch_shapes=[
             pltpu.VMEM((TOK, 2048), bf16),
@@ -431,7 +476,6 @@
         compiler_params=limit(16),
         cost_estimate=pl.CostEstimate(flops=10**9, bytes_accessed=5 * 10**6, transcendentals=0),
     )(
-        rank,
         *far(
             tokens, summary_key_weight.T, summary_value_weight.T, squeeze_key_in, squeeze_value_in,
             squeeze_key_t, squeeze_value_t, turn, chosen,
@@ -441,45 +485,25 @@
     weight_3 = around(output_weight, -1)
     arrived = lax.all_to_all(payload, "kv", 0, 0, tiled=True)
     cosine, sine = tables(kv_rank * TOK + jnp.arange(TOK, dtype=jnp.int32))
-    queries, pairs, gates, place, bound = pl.pallas_call(
-        project_kernel,
-        name="projections",
-        out_shape=(
-            stored((QB, HEADS * BLK, 128), bf16),
-            stored((TOK, 128), bf16),
-            stored((TOK, 2 * HEADS), f32),
-            stored((QB, NSEL), jnp.int32),
-            stored((QB, NSEL * BLK), f32),
-        ),
+    row_block = pl.BlockSpec((PART, 128), lambda n: (n, 0))
+    token_block = pl.BlockSpec((PART, 2048), lambda n: (n, 0))
+    pairs, gates = pl.pallas_call(
+        pair_kernel,
+        name="pairs",
+        out_shape=(stored((TOK, 128), bf16), stored((TOK, 2 * HEADS), f32)),
         grid=(TOK // PART,),
-        in_specs=[
-            SMEM,
-            pl.BlockSpec((PART, 2048), lambda n: (n, 0)),
-            VMEM, VMEM, VMEM, VMEM,
-            pl.BlockSpec((PART, 128), lambda n: (n, 0)),
-            pl.BlockSpec((PART, 128), lambda n: (n, 0)),
-            VMEM, VMEM,
-        ],
-        out_specs=(
-            pl.BlockSpec((PART // BLK, HEADS * BLK, 128), lambda n: (n, 0, 0)),
-            pl.BlockSpec((PART, 128), lambda n: (n, 0)),
-            pl.BlockSpec((PART, 2 * HEADS), lambda n: (n, 0)),
-            VMEM, VMEM,
-        ),
+        in_specs=[token_block, VMEM, VMEM, VMEM, row_block, row_block],
+        out_specs=(row_block, pl.BlockSpec((PART, 2 * HEADS), lambda n: (n, 0))),
         scratch_shapes=[pltpu.VMEM((2 * HD + 2 * HEADS, 2048), bf16)],
-        compiler_params=limit(20),
-        cost_estimate=pl.CostEstimate(flops=10**10, bytes_accessed=5 * 10**6, transcendentals=0),
-    )(
-        rank,
-        *far(tokens, query_weight, chosen_key_t, chosen_value_t),
-        gate_t, cosine, sine, chosen, code,
-    )
+        compiler_params=limit(16),
+        cost_estimate=pl.CostEstimate(flops=10**10, bytes_accessed=3 * 10**6, transcendentals=0),
+    )(*far(tokens, chosen_key_t, chosen_value_t), gate_t, *far(cosine, sine))
     picked = pl.pallas_call(
         pick_kernel,
         name="pick",
         out_shape=shape_of((PEERS, CAP * BLK, 128), bf16),
         grid=(PEERS // PICK,),
-        in_specs=[SMEM, VMEM, HBM],
+        in_specs=[VMEM, HBM],
         out_specs=pl.BlockSpec((PICK, CAP * BLK, 128), lambda step: (step, 0, 0)),
         scratch_shapes=[
             pltpu.VMEM((TOK, 128), bf16),
@@ -488,47 +512,71 @@
             pltpu.SemaphoreType.DMA((2,)),
         ],
         compiler_params=limit(8),
-    )(rank, arrived, *far(pairs))
+    )(arrived, *far(pairs))
     fetched = lax.all_to_all(picked, "kv", 0, 0, tiled=True)
-    last_cos, last_sin = tables(jnp.arange(PEERS, dtype=jnp.int32) * TOK + (TOK + CMP_STRIDE - 1))
+    queries, place, bound = pl.pallas_call(
+        query_kernel,
+        name="queries",
+        out_shape=(
+            stored((QB, HEADS * BLK, 128), bf16),
+            stored((QB, NSEL), jnp.int32),
+            stored((QB, NSEL * BLK), f32),
+        ),
+        grid=(TOK // PART,),
+        in_specs=[
+            token_block, VMEM, row_block, row_block, VMEM, VMEM,
+        ],
+        out_specs=(
+            pl.BlockSpec((PART // BLK, HEADS * BLK, 128), lambda n: (n, 0, 0)),
+            VMEM,
+            VMEM,
+        ),
+        compiler_params=limit(16),
+        cost_estimate=pl.CostEstimate(flops=10**10, bytes_accessed=3 * 10**6, transcendentals=0),
+    )(*far(tokens, query_weight, cosine, sine, chosen, code))
     mixed = pl.pallas_call(
         compressed_kernel,
         name="compressed",
         out_shape=stored((TOK, HEADS * HD), bf16),
-        in_specs=[SMEM] + [VMEM] * 7,
+        in_specs=[VMEM] * 6,
         out_specs=VMEM,
         scratch_shapes=[
             pltpu.VMEM((PEERS * NSUM, 128), bf16),
             pltpu.VMEM((PEERS * NSUM, 128), bf16),
+            pltpu.VMEM((QB * HEADS * BLK, PEERS * NSUM), f32),
+            pltpu.VMEM((QB * HEADS * BLK, PEERS * NSUM), bf16),
         ],
-        compiler_params=limit(16),
+        compiler_params=limit(24),
         cost_estimate=pl.CostEstimate(flops=10**10, bytes_accessed=3 * 10**6, transcendentals=0),
-    )(rank, arrived, *far(queries, gates), squeeze_key_t, squeeze_value_t, last_cos, last_sin)
-    weight_1, mixed = lax.optimization_barrier((weight_1, mixed))
-    weight_2 = around(weight_1, 1)
-
+    )(arrived, *far(queries, gates, squeeze_key_t, squeeze_value_t, turn))
+    weight_1, weight_3, mixed = lax.optimization_barrier((weight_1, weight_3, mixed))
+    half = weight_1.shape[0] // 2
+    weight_2a = around(weight_1[:half], 1)
+    weight_2b = around(weight_3[half:], -1)
     pieces = pl.pallas_call(
         selected_kernel,
         name="selected",
         out_shape=(shape_of((PER_CHIP * BLK, HEADS * HD), bf16),) * CHIPS,
-        in_specs=[SMEM, SMEM] + [HBM] * 6,
+        in_specs=[HBM] * 7,
         out_specs=(VMEM,) * CHIPS,
         scratch_shapes=[
+            pltpu.SMEM((QB, NSEL), jnp.int32),
             pltpu.VMEM((PEERS * CAP * BLK, 128), bf16),
             pltpu.VMEM((TOK, 128), bf16),
             pltpu.VMEM((QB, HEADS * BLK, 128), bf16),
+            pltpu.VMEM((QB, NSEL * BLK), f32),
             pltpu.VMEM((TOK, 2 * HEADS), f32),
             pltpu.VMEM((TOK, HEADS * HD), bf16),
-            pltpu.VMEM((QB, NSEL * BLK), f32),
-            pltpu.VMEM((PER_CHIP, NSEL * BLK, 128), bf16),
+            pltpu.VMEM((QB, NSEL * BLK, 128), bf16),
+            pltpu.VMEM((QB, HEADS * BLK, NSEL * BLK), f32),
+            pltpu.VMEM((QB, HEADS * BLK, NSEL * BLK), bf16),
             pltpu.VMEM((CHIPS, PER_CHIP * BLK, HEADS * HD), bf16),
-            pltpu.SemaphoreType.DMA((6,)),
+            pltpu.SemaphoreType.DMA((7,)),
         ],
-        compiler_params=limit(16),
+        compiler_params=limit(24),
         cost_estimate=pl.CostEstimate(flops=10**9, bytes_accessed=3 * 10**6, transcendentals=0),
     )(
-        rank, place,
-        *far(fetched.reshape(PEERS * CAP * BLK, 128), pairs, queries, gates, mixed, bound),
+        *far(place, fetched.reshape(PEERS * CAP * BLK, 128), pairs, queries, bound, gates, mixed),
     )
     piece_2 = around(pieces[2], 2)
     piece_1 = around(pieces[1], 1)
@@ -537,12 +585,13 @@
         output_kernel,
         name="output",
         out_shape=(shape_of((OUT_ROWS, 2048), f32), shape_of((OUT_ROWS, 2048), bf16)),
-        in_specs=[SMEM] + [VMEM] * 8,
+        in_specs=[VMEM] * 9,
         out_specs=(VMEM, VMEM),
         scratch_shapes=[pltpu.VMEM((2 * OUT_ROWS, 2048), f32)],
         compiler_params=limit(16),
     )(
-        rank, pieces[0], piece_1, piece_2, piece_3, output_weight, weight_1, weight_2, weight_3,
+        pieces[0], piece_1, piece_2, piece_3, output_weight, weight_1, weight_2a, weight_2b,
+        weight_3,
     )
     swapped = lax.ppermute(other, "tp", [(i, i ^ 1) for i in range(2 * CHIPS)])
     return (mine + swapped.astype(f32)).astype(bf16)

time: 89.8 us -> 85.3 us (0.950)
  Pallas kernels: 35.1 us -> 31 us
  waiting for transfers between devices: 22.7 us -> 18.9 us
  local copies, waits for them, and re-layouts: 0.03 us -> 1.68 us
  starting transfers between devices: 29.3 us -> 30.7 us
    all_to_all x1, waiting for transfers between devices: 14.7 us -> 8.68 us  [on_device(): fetched = lax.all_to_all(picked, 'kv', 0, 0, tiled=True)]
    pallas_call x1, Pallas kernels: 8.54 us -> 5.73 us  [on_device(): pl.pallas_call(selected_kernel, name='selected', out_shape=(shape_of((PER...]
    all_to_all x1, waiting for transfers between devices: 4.85 us -> 6.97 us  [on_device(): arrived = lax.all_to_all(payload, 'kv', 0, 0, tiled=True)]
    pallas_call x1 -> x2, Pallas kernels: 6.17 us -> 7.97 us  [the longest x1 4.7 us: on_device(): pl.pallas_call(query_kernel, name='queries', out_shape=(stored((QB, HEADS...]
    slice x0 -> x2, local copies, waits for them, and re-layouts: none -> 1.67 us  [the longest x1 0.83 us: on_device(): weight_2b = around(weight_3[half:], -1)]
    pallas_call x1, Pallas kernels: 10.3 us -> 8.71 us  [on_device(): pl.pallas_call(compressed_kernel, name='compressed', out_shape=stored((TO...]
    ppermute x6 -> x7, starting transfers between devices: 7.37 us -> 8.83 us  [around(): return lax.ppermute(value, 'tp', route)]
    pallas_call x1, Pallas kernels: 3.27 us -> 2.18 us  [on_device(): pl.pallas_call(pick_kernel, name='pick', out_shape=shape_of((PEERS, CAP *...]
  transfers between devices with their start and end apart: 9 -> 10, of which waited for: 6 -> 6; matrix products, arithmetic and copies ran while one was open for 1% -> 4% of each run, Pallas kernels for 37% -> 34%
where the time goes in v1:
time: 85.3 us; the launch traced here: 85 us
  Pallas kernels  31 us (36%)
  starting transfers between devices  30.7 us (36%)
  waiting for transfers between devices  18.9 us (22%)
  other arithmetic  2.58 us (3%)
  local copies, waits for them, and re-layouts  1.68 us (2%)
    all_to_all x1, starting transfers between devices, on_device(): arrived = lax.all_to_all(payload, 'kv', 0, 0, tiled=True)  11 us
    ppermute x7, starting transfers between devices, around(): return lax.ppermute(value, 'tp', route)  8.83 us
    pallas_call x1, Pallas kernels, on_device(): pl.pallas_call(compressed_kernel, name='compressed', out_shape=stored((TO...  8.71 us
    all_to_all x1, waiting for transfers between devices, on_device(): fetched = lax.all_to_all(picked, 'kv', 0, 0, tiled=True)  8.68 us
    all_to_all x1, waiting for transfers between devices, on_device(): arrived = lax.all_to_all(payload, 'kv', 0, 0, tiled=True)  6.97 us
    pallas_call x1, Pallas kernels, on_device(): pl.pallas_call(selected_kernel, name='selected', out_shape=(shape_of((PER...  5.73 us
    ppermute x1, starting transfers between devices, on_device(): swapped = lax.ppermute(other, 'tp', [(i, i ^ 1) for i in range(2 * CHIPS)])  5.52 us
    all_to_all x1, starting transfers between devices, on_device(): fetched = lax.all_to_all(picked, 'kv', 0, 0, tiled=True)  5.33 us
  transfers between devices with their start and end apart: 10, of which 6 were waited for; matrix products, arithmetic and copies ran while one was open for 4% of the time, Pallas kernels for 34%

profile of v1, /device:TPU:1, one launch (start us, length us, event | category | flops | bytes accessed | tf_op | source)
XLA Modules:
  0.0 85.0 jit_solution(4952361097882422612)
XLA Ops:
  0.0 2.1 %collective-permute-start = (bf16[256,2048]{1,0:T(8,128)(2,1)}, bf16[256,2048]{1,0:T(8,128)(2,1)S(1)}, u32[]{:S(2)}, u32[]{:S(2)}) collective-permute-start(bf16[256,2048]{1,0:T(8,128)(2,1)} %w0_ref.1), channel_id=1, source_target_pairs={{0,2},{1,3},{2,4},{3,5},{4,6},{5,7},{6,0},{7,1},{8,10},{9,11},{10,... | collective-permute-start | bytes 3145736 | tf_op jit(solution)/shard_map/ppermute | solution.py:437
  2.1 1.4 %collective-permute-start.1 = (bf16[256,2048]{1,0:T(8,128)(2,1)}, bf16[256,2048]{1,0:T(8,128)(2,1)S(1)}, u32[]{:S(2)}, u32[]{:S(2)}) collective-permute-start(bf16[256,2048]{1,0:T(8,128)(2,1)} %w0_ref.1), channel_id=1, source_target_pairs={{0,6},{1,7},{2,0},{3,1},{4,2},{5,3},{6,4},{7,5},{8,14},{9,15},{10,... | collective-permute-start | bytes 3145736 | tf_op jit(solution)/shard_map/ppermute | solution.py:437
  3.6 4.3 %summaries.1 = (bf16[32,40,128]{2,1,0:T(8,128)(2,1)}, f32[8,512]{1,0:T(8,128)}) custom-call(bf16[512,2048]{1,0:T(8,128)(2,1)} %tokens_ref.3, bf16[64,2048]{1,0:T(8,128)(2,1)} %bitcast.10, bf16[64,2048]{1,0:T(8,128)(2,1)} %bitcast.11, bf16[2048,128]{1,0:T(8,128)(2,1)} %ink_hbm.1, bf16[2048,128]{1,0:T(8,128)(2,1)} %inv_hbm.1, bf16[64,128]{1,0:T(8,128)(2,1)} %bitcast.12, ...), custom_call_target="tpu_custom_call" | custom-call | flops 1000000000 | bytes 5000000 | tf_op jit(solution)/shard_map/summaries/pallas_call | solution.py:458
  7.8 11.0 %all-to-all-start = ((bf16[32,40,128]{2,1,0:T(8,128)(2,1)}), bf16[32,40,128]{2,1,0:T(8,128)(2,1)S(1)}, u32[]{:S(2)}, u32[]{:S(2)}) async-start(bf16[32,40,128]{2,1,0:T(8,128)(2,1)} %get-tuple-element.23), calls=%async_computation | async-start | bytes 655360 | tf_op jit(solution)/shard_map/all_to_all | solution.py:486
  18.9 1.8 %fusion = (f32[512,128]{1,0:T(8,128)}, f32[512,128]{1,0:T(8,128)}) fusion(f32[128]{0:T(128)S(1)} %copy-done.2, f32[128]{0:T(128)S(1)} %copy-done.3, f32[512]{0:T(512)S(1)} %add_convert_fusion.1), kind=kLoop, calls=%fused_computation.3 | loop fusion | flops 131072 | bytes 527360 | tf_op jit(solution)/shard_map/mul | solution.py:442
  20.8 3.3 %pairs.1 = (bf16[512,128]{1,0:T(8,128)(2,1)}, f32[512,8]{1,0:T(8,128)}) custom-call(bf16[512,2048]{1,0:T(8,128)(2,1)} %tokens_ref.3, bf16[64,2048]{1,0:T(8,128)(2,1)} %bitcast.18, bf16[64,2048]{1,0:T(8,128)(2,1)} %bitcast.19, bf16[2,4,2048]{2,1,0:T(4,128)(2,1)S(1)} %bitcast.9, f32[512,128]{1,0:T(8,128)} %get-tuple-element.38.cos_ref, ...), custom_call_target="tpu_custom_call" | custom-call | flops 10000000000 | bytes 3000000 | tf_op jit(solution)/shard_map/pairs/pallas_call | solution.py:490
  24.0 7.0 %all-to-all-done.arrived_ref = bf16[32,40,128]{2,1,0:T(8,128)(2,1)S(1)} async-done(((bf16[32,40,128]{2,1,0:T(8,128)(2,1)}), bf16[32,40,128]{2,1,0:T(8,128)(2,1)S(1)}, u32[]{:S(2)}, u32[]{:S(2)}) %all-to-all-start) | async-done | bytes 327712 | tf_op jit(solution)/shard_map/all_to_all | solution.py:486
  31.0 2.2 %pick.1 = bf16[32,128,128]{2,1,0:T(8,128)(2,1)} custom-call(bf16[32,40,128]{2,1,0:T(8,128)(2,1)S(1)} %all-to-all-done.arrived_ref, bf16[512,128]{1,0:T(8,128)(2,1)} %get-tuple-element.24.pair_hbm), custom_call_target="tpu_custom_call" | custom-call | tf_op jit(solution)/shard_map/pick/pallas_call | solution.py:501
  33.2 5.3 %all-to-all-start.1 = ((bf16[32,128,128]{2,1,0:T(8,128)(2,1)}), bf16[32,128,128]{2,1,0:T(8,128)(2,1)}, u32[]{:S(2)}, u32[]{:S(2)}) async-start(bf16[32,128,128]{2,1,0:T(8,128)(2,1)} %pick.1), calls=%async_computation.1 | async-start | bytes 2097152 | tf_op jit(solution)/shard_map/all_to_all | solution.py:516
  38.5 4.7 %queries.1 = (bf16[16,128,128]{2,1,0:T(8,128)(2,1)}, s32[16,16]{1,0:T(8,128)}, f32[16,512]{1,0:T(8,128)}) custom-call(bf16[512,2048]{1,0:T(8,128)(2,1)} %tokens_ref.3, bf16[2048,256]{1,0:T(8,128)(2,1)} %wq_ref.1, f32[512,128]{1,0:T(8,128)} %get-tuple-element.38.cos_ref, f32[512,128]{1,0:T(8,128)} %get-tuple-element.37.sin_ref, s32[16,16]{1,0:T(8,128)} %bitcast.17, ...), custom_call_target="tpu_custom_call" | custom-call | flops 10000000000 | bytes 3000000 | tf_op jit(solution)/shard_map/queries/pallas_call | solution.py:517
  43.2 8.7 %compressed.1.mixed_hbm = bf16[512,256]{1,0:T(8,128)(2,1)} custom-call(bf16[32,40,128]{2,1,0:T(8,128)(2,1)S(1)} %all-to-all-done.arrived_ref, bf16[16,128,128]{2,1,0:T(8,128)(2,1)} %get-tuple-element.25.query_ref.query_hbm, f32[512,8]{1,0:T(8,128)} %get-tuple-element.27.gates_ref.gates_hbm, bf16[64,128]{1,0:T(8,128)(2,1)} %bitcast.13, ...), custom_call_target="tpu_custom_call" | custom-call | flops 10000000000 | bytes 3000000 | tf_op jit(solution)/shard_map/compressed/pallas_call | solution.py:537
  51.9 0.0 collective-permute-done.w1_ref
  51.9 0.0 collective-permute-done.1.w3_ref
  51.9 0.8 slice.6
  52.8 0.8 slice.7
  53.6 1.5 %collective-permute-start.6 = (bf16[128,2048]{1,0:T(8,128)(2,1)}, bf16[128,2048]{1,0:T(8,128)(2,1)}, u32[]{:S(2)}, u32[]{:S(2)}) collective-permute-start(bf16[128,2048]{1,0:T(8,128)(2,1)} %slice.7), channel_id=1, source_target_pairs={{0,6},{1,7},{2,0},{3,1},{4,2},{5,3},{6,4},{7,5},{8,14},{9,15},{10,... | collective-permute-start | bytes 1572872 | tf_op jit(solution)/shard_map/ppermute | solution.py:437
  55.1 0.0 collective-permute-start.5
  55.1 8.7 %all-to-all-done.1 = bf16[32,128,128]{2,1,0:T(8,128)(2,1)} async-done(((bf16[32,128,128]{2,1,0:T(8,128)(2,1)}), bf16[32,128,128]{2,1,0:T(8,128)(2,1)}, u32[]{:S(2)}, u32[]{:S(2)}) %all-to-all-start.1) | async-done | bytes 1048608 | tf_op jit(solution)/shard_map/all_to_all | solution.py:516
  63.8 5.7 %selected.1 = (bf16[128,256]{1,0:T(8,128)(2,1)S(1)}, bf16[128,256]{1,0:T(8,128)(2,1)S(1)}, bf16[128,256]{1,0:T(8,128)(2,1)S(1)}, bf16[128,256]{1,0:T(8,128)(2,1)S(1)}) custom-call(s32[16,16]{1,0:T(8,128)} %get-tuple-element.22.place_hbm, bf16[4096,128]{1,0:T(8,128)(2,1)} %bitcast.8.fetched_hbm, bf16[512,128]{1,0:T(8,128)(2,1)} %get-tuple-element.24.pair_hbm, ...), custom_call_target="tpu_custom_call" | custom-call | flops 1000000000 | bytes 3000000 | tf_op jit(solution)/shard_map/selected/pallas_call | solution.py:556
  69.5 0.1 collective-permute-start.2
  69.6 2.6 %collective-permute-start.3 = (bf16[128,256]{1,0:T(8,128)(2,1)S(1)}, bf16[128,256]{1,0:T(8,128)(2,1)S(1)}, u32[]{:S(2)}, u32[]{:S(2)}) collective-permute-start(bf16[128,256]{1,0:T(8,128)(2,1)S(1)} %get-tuple-element.31), channel_id=1, source_target_pairs={{0,4},{1,5},{2,6},{3,7},{4,0},{5,1},{6,2},{7,3},{8,12},{9,13},{10,... | collective-permute-start | bytes 196616 | tf_op jit(solution)/shard_map/ppermute | solution.py:437
  72.2 1.1 %collective-permute-start.4 = (bf16[128,256]{1,0:T(8,128)(2,1)S(1)}, bf16[128,256]{1,0:T(8,128)(2,1)S(1)}, u32[]{:S(2)}, u32[]{:S(2)}) collective-permute-start(bf16[128,256]{1,0:T(8,128)(2,1)S(1)} %get-tuple-element.32), channel_id=1, source_target_pairs={{0,6},{1,7},{2,0},{3,1},{4,2},{5,3},{6,4},{7,5},{8,14},{9,15},{10,... | collective-permute-start | bytes 196616 | tf_op jit(solution)/shard_map/ppermute | solution.py:437
  73.3 0.0 collective-permute-done.6.w2b_ref
  73.3 0.0 collective-permute-done.5.w2a_ref
  73.3 0.6 collective-permute-done.2.a1_ref
  73.9 0.7 collective-permute-done.3.a2_ref
  74.6 0.7 collective-permute-done.4.a3_ref
  75.4 0.0 copy-done
  75.4 2.2 %output.1 = (f32[64,2048]{1,0:T(8,128)S(1)}, bf16[64,2048]{1,0:T(8,128)(2,1)S(1)}) custom-call(bf16[128,256]{1,0:T(8,128)(2,1)S(1)} %get-tuple-element.29.a0_ref, bf16[128,256]{1,0:T(8,128)(2,1)S(1)} %collective-permute-done.2.a1_ref, bf16[128,256]{1,0:T(8,128)(2,1)S(1)} %collective-permute-done.3.a2_ref, ...), custom_call_target="tpu_custom_call" | custom-call | tf_op jit(solution)/shard_map/output/pallas_call | solution.py:584
  77.5 5.5 %collective-permute-start.7 = (bf16[64,2048]{1,0:T(8,128)(2,1)S(1)}, bf16[64,2048]{1,0:T(8,128)(2,1)S(1)}, u32[]{:S(2)}, u32[]{:S(2)}) collective-permute-start(bf16[64,2048]{1,0:T(8,128)(2,1)S(1)} %get-tuple-element.36), channel_id=1, source_target_pairs={{0,1},{1,0},{2,3},{3,2},{4,5},{5,4},{6,7},{7,6},{8,9},{9,8},{10,11... | collective-permute-start | bytes 786440 | tf_op jit(solution)/shard_map/ppermute | solution.py:596
  83.0 1.2 %collective-permute-done.7 = bf16[64,2048]{1,0:T(8,128)(2,1)S(1)} collective-permute-done((bf16[64,2048]{1,0:T(8,128)(2,1)S(1)}, bf16[64,2048]{1,0:T(8,128)(2,1)S(1)}, u32[]{:S(2)}, u32[]{:S(2)}) %collective-permute-start.7) | collective-permute-done | bytes 262176 | tf_op jit(solution)/shard_map/ppermute | solution.py:596
  84.2 0.8 add_convert_fusion
  (8 shorter events, 0.0 us)
Async XLA Ops:
  0.0 51.9 %collective-permute-start = (bf16[256,2048]{1,0:T(8,128)(2,1)}, bf16[256,2048]{1,0:T(8,128)(2,1)S(1)}, u32[]{:S(2)}, u32[]{:S(2)}) collective-permute-start(bf16[256,2048]{1,0:T(8,128)(2,1)} %w0_ref.1), channel_id=1, source_target_pairs={{0,2},{1,3},{2,4},{3,5},{4,6},{5,7},{6,0},{7,1},{8,10},{9,11},{10,... | collective-permute-start | bytes 3145736 | tf_op jit(solution)/shard_map/ppermute | solution.py:437
  2.1 49.8 %collective-permute-start.1 = (bf16[256,2048]{1,0:T(8,128)(2,1)}, bf16[256,2048]{1,0:T(8,128)(2,1)S(1)}, u32[]{:S(2)}, u32[]{:S(2)}) collective-permute-start(bf16[256,2048]{1,0:T(8,128)(2,1)} %w0_ref.1), channel_id=1, source_target_pairs={{0,6},{1,7},{2,0},{3,1},{4,2},{5,3},{6,4},{7,5},{8,14},{9,15},{10,... | collective-permute-start | bytes 3145736 | tf_op jit(solution)/shard_map/ppermute | solution.py:437
  3.6 15.4 %copy-start.2 = (f32[128]{0:T(128)S(1)}, f32[128]{0:T(128)}, u32[]{:S(2)}) copy-start(f32[128]{0:T(128)} %constant.20) | copy-start | bytes 1540
  3.6 15.4 %copy-start.3 = (f32[128]{0:T(128)S(1)}, f32[128]{0:T(128)}, u32[]{:S(2)}) copy-start(f32[128]{0:T(128)} %constant.19) | copy-start | bytes 1540
  3.6 17.2 %copy-start.1 = (bf16[2,2048,4]{1,2,0:T(4,128)(2,1)S(1)}, bf16[2,2048,4]{1,2,0:T(4,128)(2,1)}, u32[]{:S(2)}) copy-start(bf16[2,2048,4]{1,2,0:T(4,128)(2,1)} %param.26) | copy-start | bytes 98308
  7.8 23.2 %all-to-all-start = ((bf16[32,40,128]{2,1,0:T(8,128)(2,1)}), bf16[32,40,128]{2,1,0:T(8,128)(2,1)S(1)}, u32[]{:S(2)}, u32[]{:S(2)}) async-start(bf16[32,40,128]{2,1,0:T(8,128)(2,1)} %get-tuple-element.23), calls=%async_computation | async-start | bytes 655360 | tf_op jit(solution)/shard_map/all_to_all | solution.py:486
  33.2 30.6 %all-to-all-start.1 = ((bf16[32,128,128]{2,1,0:T(8,128)(2,1)}), bf16[32,128,128]{2,1,0:T(8,128)(2,1)}, u32[]{:S(2)}, u32[]{:S(2)}) async-start(bf16[32,128,128]{2,1,0:T(8,128)(2,1)} %pick.1), calls=%async_computation.1 | async-start | bytes 2097152 | tf_op jit(solution)/shard_map/all_to_all | solution.py:516
  53.6 21.8 %copy-start = (bf16[256,2048]{1,0:T(8,128)(2,1)S(1)}, bf16[256,2048]{1,0:T(8,128)(2,1)}, u32[]{:S(2)}) copy-start(bf16[256,2048]{1,0:T(8,128)(2,1)} %w0_ref.1) | copy-start | bytes 3145732
  53.6 19.7 %collective-permute-start.6 = (bf16[128,2048]{1,0:T(8,128)(2,1)}, bf16[128,2048]{1,0:T(8,128)(2,1)}, u32[]{:S(2)}, u32[]{:S(2)}) collective-permute-start(bf16[128,2048]{1,0:T(8,128)(2,1)} %slice.7), channel_id=1, source_target_pairs={{0,6},{1,7},{2,0},{3,1},{4,2},{5,3},{6,4},{7,5},{8,14},{9,15},{10,... | collective-permute-start | bytes 1572872 | tf_op jit(solution)/shard_map/ppermute | solution.py:437
  55.1 18.2 %collective-permute-start.5 = (bf16[128,2048]{1,0:T(8,128)(2,1)}, bf16[128,2048]{1,0:T(8,128)(2,1)}, u32[]{:S(2)}, u32[]{:S(2)}) collective-permute-start(bf16[128,2048]{1,0:T(8,128)(2,1)} %slice.6), channel_id=1, source_target_pairs={{0,2},{1,3},{2,4},{3,5},{4,6},{5,7},{6,0},{7,1},{8,10},{9,11},{10,... | collective-permute-start | bytes 1572872 | tf_op jit(solution)/shard_map/ppermute | solution.py:437
  69.5 4.4 %collective-permute-start.2 = (bf16[128,256]{1,0:T(8,128)(2,1)S(1)}, bf16[128,256]{1,0:T(8,128)(2,1)S(1)}, u32[]{:S(2)}, u32[]{:S(2)}) collective-permute-start(bf16[128,256]{1,0:T(8,128)(2,1)S(1)} %get-tuple-element.30), channel_id=1, source_target_pairs={{0,2},{1,3},{2,4},{3,5},{4,6},{5,7},{6,0},{7,1},{8,10},{9,11},{10,... | collective-permute-start | bytes 196616 | tf_op jit(solution)/shard_map/ppermute | solution.py:437
  69.6 5.0 %collective-permute-start.3 = (bf16[128,256]{1,0:T(8,128)(2,1)S(1)}, bf16[128,256]{1,0:T(8,128)(2,1)S(1)}, u32[]{:S(2)}, u32[]{:S(2)}) collective-permute-start(bf16[128,256]{1,0:T(8,128)(2,1)S(1)} %get-tuple-element.31), channel_id=1, source_target_pairs={{0,4},{1,5},{2,6},{3,7},{4,0},{5,1},{6,2},{7,3},{8,12},{9,13},{10,... | collective-permute-start | bytes 196616 | tf_op jit(solution)/shard_map/ppermute | solution.py:437
  72.2 3.1 %collective-permute-start.4 = (bf16[128,256]{1,0:T(8,128)(2,1)S(1)}, bf16[128,256]{1,0:T(8,128)(2,1)S(1)}, u32[]{:S(2)}, u32[]{:S(2)}) collective-permute-start(bf16[128,256]{1,0:T(8,128)(2,1)S(1)} %get-tuple-element.32), channel_id=1, source_target_pairs={{0,6},{1,7},{2,0},{3,1},{4,2},{5,3},{6,4},{7,5},{8,14},{9,15},{10,... | collective-permute-start | bytes 196616 | tf_op jit(solution)/shard_map/ppermute | solution.py:437
  77.5 6.7 %collective-permute-start.7 = (bf16[64,2048]{1,0:T(8,128)(2,1)S(1)}, bf16[64,2048]{1,0:T(8,128)(2,1)S(1)}, u32[]{:S(2)}, u32[]{:S(2)}) collective-permute-start(bf16[64,2048]{1,0:T(8,128)(2,1)S(1)} %get-tuple-element.36), channel_id=1, source_target_pairs={{0,1},{1,0},{2,3},{3,2},{4,5},{5,4},{6,7},{7,6},{8,9},{9,8},{10,11... | collective-permute-start | bytes 786440 | tf_op jit(solution)/shard_map/ppermute | solution.py:596

commit v2 on v1

--- a/solution.py
+++ b/solution.py
@@ -4,6 +4,7 @@
 from jax import lax
 from jax.experimental import pallas as pl
 from jax.experimental.pallas import tpu as pltpu
+from jax.sharding import Mesh
 from jax.sharding import PartitionSpec as P
 
 
@@ -17,6 +18,8 @@
 FLOOR = -1e29
 TOK = 512
 PEERS = 32
+LAYERS = 8
+COLUMNS = 4
 NSUM = 32
 ROWS = 40
 QB = TOK // BLK
@@ -27,8 +30,8 @@
 CHIPS = 4
 PER_CHIP = QB // CHIPS
 CHUNKS = 2
-PICK = 16
 PART = 256
+SPLIT = 288
 GATHERED = 8
 WEIGHED = 4
 MIXED = 8
@@ -40,6 +43,10 @@
 
 bf16 = jnp.bfloat16
 f32 = jnp.float32
+
+
+def kv_index():
+    return lax.axis_index("z") * COLUMNS + lax.axis_index("x")
 
 
 def dot(a, b):
@@ -83,28 +90,46 @@
     return jnp.where(lanes_of(both.shape) < HD, turned(both, cosine, sine), both)
 
 
-def summary_kernel(
-    tokens_hbm, wk_hbm, wv_hbm, ink_hbm, inv_hbm, outk_hbm, outv_hbm, turn_hbm, chosen_hbm,
-    payload_ref, code_ref,
-    tokens_ref, weight_ref, ink_ref, inv_ref, outk_ref, outv_ref, turn_ref, chosen_ref, raw_ref, sems,
+def token_kernel(
+    tokens_hbm, wk_hbm, wv_hbm, ck_hbm, cv_hbm, ink_hbm, inv_hbm, outk_hbm, outv_hbm, turn_hbm,
+    chosen_hbm, payload_ref, code_ref, cos_ref, sin_ref,
+    tokens_ref, weight_ref, ink_ref, inv_ref, outk_ref, outv_ref, turn_ref, chosen_ref, raw_ref,
+    coarse_ref, sems,
 ):
-    rank = lax.axis_index("kv")
+    rank = kv_index()
     part = TOK // CHUNKS
     copies = [
         (chosen_hbm, chosen_ref),
+        (turn_hbm, turn_ref),
         (wk_hbm, weight_ref.at[:HD]),
-        (wv_hbm, weight_ref.at[HD:]),
+        (wv_hbm, weight_ref.at[HD : 2 * HD]),
+        (ck_hbm, weight_ref.at[2 * HD : 3 * HD]),
+        (cv_hbm, weight_ref.at[3 * HD :]),
         *((tokens_hbm.at[pl.ds(c * part, part)], tokens_ref.at[pl.ds(c * part, part)]) for c in range(CHUNKS)),
         (ink_hbm, ink_ref),
         (inv_hbm, inv_ref),
         (outk_hbm, outk_ref),
         (outv_hbm, outv_ref),
-        (turn_hbm, turn_ref),
     ]
     copies = [pltpu.make_async_copy(a, b, sems.at[n]) for n, (a, b) in enumerate(copies)]
     for copy in copies:
         copy.start()
     copies[0].wait()
+    copies[1].wait()
+    inverse = turn_ref[:1]
+    groups = TOK // 8
+    angles = (rank * TOK + 8 * rows_of((groups, 128))).astype(f32) * inverse
+    coarse_ref[0] = jnp.cos(angles)
+    coarse_ref[1] = jnp.sin(angles)
+    angles = rows_of((8, 128)).astype(f32) * inverse
+    fine_cos = jnp.cos(angles)
+    fine_sin = jnp.sin(angles)
+    for group in range(groups):
+        cosine = coarse_ref[0, group : group + 1, :]
+        sine = coarse_ref[1, group : group + 1, :]
+        rows = slice(8 * group, 8 * group + 8)
+        cos_ref[rows, :] = cosine * fine_cos - sine * fine_sin
+        sin_ref[rows, :] = (sine * fine_cos + cosine * fine_sin) * turn_ref[1:]
     chosen = chosen_ref[...]
     query_block = rank * QB + rows_of(chosen.shape)
     wanted = jnp.where((chosen <= query_block) & (chosen // QB != rank), chosen, -1)
@@ -117,15 +142,19 @@
     running = present
     for step in (1, 2, 4, 8):
         running = running + jnp.where(lane % QB >= step, pltpu.roll(running, step, 1), 0.0)
-    code = jnp.where(present > 0.0, running - present, UNUSED)
-    code_ref[...] = code
-    copies[1].wait()
-    copies[2].wait()
+    code_ref[...] = jnp.where(present > 0.0, running - present, UNUSED)
+    for copy in copies[2:6]:
+        copy.wait()
     for c in range(CHUNKS):
-        copies[3 + c].wait()
+        copies[6 + c].wait()
         rows = slice(c * part, c * part + part)
-        raw_ref[rows] = dot_t(tokens_ref[rows], weight_ref[...]).astype(bf16).astype(f32)
-    for copy in copies[3 + CHUNKS :]:
+        four = dot_t(tokens_ref[rows], weight_ref[...])
+        raw_ref[rows] = four[:, :128].astype(bf16).astype(f32)
+        pair = four[:, 128:]
+        lane = lanes_of(pair.shape)
+        pair = jnp.where(lane < HD, turned(pair, cos_ref[rows, :], sin_ref[rows, :]), pair).astype(bf16)
+        payload_ref[rows, :] = pair
+    for copy in copies[6 + CHUNKS :]:
         copy.wait()
     ends = (rank * NSUM + rows_of((NSUM, 128))) * CMP_STRIDE + 2 * CMP_STRIDE - 1
     cosine, sine = turns(ends, turn_ref)
@@ -145,46 +174,20 @@
     low_v, high_v = total[:, 256:384], total[:, 384:]
     pre_k = low_k + pltpu.roll(high_k, NSUM - 1, 0)
     pre_v = low_v + pltpu.roll(high_v, NSUM - 1, 0)
-    summaries = squeeze_out(
-        pre_k, pre_v, outk_ref[...], outv_ref[...], cosine, sine
-    )
-    payload = jnp.concatenate(
-        [
-            summaries,
-            low_k[NSUM - 1 :], low_v[NSUM - 1 :], high_k[:1], high_v[:1],
-            code[:1, :128], code[:1, 128:256], code[:1, 256:384], code[:1, 384:],
-        ],
-        0,
-    ).astype(bf16)
-    for peer in range(PEERS):
-        payload_ref[peer] = payload
-
-
-def pair_kernel(
-    tokens_ref, wk_ref, wv_ref, gate_ref, cos_ref, sin_ref, pair_ref, gates_ref, weight_ref
+    summaries = squeeze_out(pre_k, pre_v, outk_ref[...], outv_ref[...], cosine, sine)
+    edges = [low_k[NSUM - 1 :], low_v[NSUM - 1 :], high_k[:1], high_v[:1]]
+    rest = jnp.zeros((ROWS - NSUM - 4, 128), f32)
+    extra = jnp.concatenate([summaries, *edges, rest], 0).astype(bf16)
+    payload_ref[TOK:, :] = extra
+
+
+def query_kernel(
+    tokens_ref, wq_ref, gate_ref, cos_ref, sin_ref, chosen_ref, code_ref,
+    query_ref, gates_ref, place_ref, bound_ref,
 ):
     @pl.when(pl.program_id(0) == 0)
     def _():
-        weight_ref[:HD] = wk_ref[...]
-        weight_ref[HD : 2 * HD] = wv_ref[...]
-        weight_ref[2 * HD :] = jnp.concatenate([gate_ref[0], gate_ref[1]], 0)
-
-    both = dot_t(tokens_ref[...], weight_ref[...])
-    pair = both[:, : 2 * HD]
-    lane = lanes_of(pair.shape)
-    pair_ref[...] = jnp.where(
-        lane < HD, turned(pair, cos_ref[...], sin_ref[...]), pair
-    ).astype(bf16)
-    gates_ref[...] = jax.nn.sigmoid(both[:, 2 * HD :])
-
-
-def query_kernel(
-    tokens_ref, wq_ref, cos_ref, sin_ref, chosen_ref, code_ref,
-    query_ref, place_ref, bound_ref,
-):
-    @pl.when(pl.program_id(0) == 0)
-    def _():
-        rank = lax.axis_index("kv")
+        rank = kv_index()
         chosen = chosen_ref[...]
         query_block = rank * QB + rows_of(chosen.shape)
         code = code_ref[...]
@@ -196,8 +199,9 @@
             found = jnp.where(every == chosen[:, k : k + 1], code, 0.0)
             slot = jnp.where(slot_lane == k, jnp.sum(found, 1, keepdims=True), slot)
         holder = chosen // QB
+        arrival = holder % COLUMNS * LAYERS + holder // COLUMNS
         place = jnp.where(
-            holder == rank, PEERS * CAP + chosen % QB, holder * CAP + slot.astype(jnp.int32)
+            holder == rank, PEERS * CAP + chosen % QB, arrival * CAP + slot.astype(jnp.int32)
         )
         place_ref[...] = jnp.where(chosen <= query_block, place, PEERS * CAP)
         order = jnp.where(chosen < query_block, -1.0, jnp.where(chosen > query_block, 1.0, 0.0))
@@ -208,6 +212,8 @@
     cosine = cos_ref[...]
     sine = sin_ref[...]
     lane = lanes_of(cosine.shape)
+    gate = jnp.concatenate([gate_ref[0], gate_ref[1]], 0)
+    gates_ref[...] = jax.nn.sigmoid(dot_t(tokens_ref[...], gate))
     queries = dot(tokens_ref[...], wq_ref[...]) * np.float32(HD ** -0.5)
     for side in range(2):
         both = turned(queries[:, 128 * side : 128 * side + 128], cosine, sine)
@@ -219,35 +225,45 @@
                 query_ref[b, head * BLK : (head + 1) * BLK, :] = one[b * BLK : (b + 1) * BLK]
 
 
-def pick_kernel(arrived_ref, pair_hbm, picked_ref, pair_ref, ids_ref, ids_smem, sems):
-    rank = lax.axis_index("kv")
-    step = pl.program_id(0)
-
-    @pl.when(step == 0)
+def pick_kernel(
+    code0_ref, code1_ref, code2_ref, code3_ref, own_ref, up1_ref, up2_ref, up3_ref, far_a_ref,
+    far_b_ref, down3_ref, down2_ref, down1_ref, picked_ref, column_ref,
+    far_ref, code_ref, ids_ref, ids_smem, sem,
+):
+    asker = pl.program_id(0)
+    place = lax.axis_index("z")
+    stock = (own_ref, up1_ref, up2_ref, up3_ref, far_ref, down3_ref, down2_ref, down1_ref)
+
+    @pl.when(asker == 0)
     def _():
-        load = pltpu.make_async_copy(pair_hbm, pair_ref, sems.at[0])
-        load.start()
-        flat = arrived_ref[...].reshape(PEERS * ROWS, 128)
-        shape = (PEERS, PEERS * ROWS)
-        chosen_row = (lanes_of(shape) == rows_of(shape) * ROWS + NSUM + 4 + rank // 8).astype(bf16)
-        codes = dot(chosen_row, flat)
-        lane = lanes_of((PEERS, 128))
-        mine = lane // QB == rank % 8
+        column = lax.axis_index("x")
+        for d, ref in enumerate((code0_ref, code1_ref, code2_ref, code3_ref)):
+            code_ref[(column - d + COLUMNS) % COLUMNS] = ref[...]
+        lane = lanes_of((LAYERS, NBLK))
+        mine = lane // QB == rows_of((LAYERS, NBLK)) * COLUMNS + column
         inner = (lane % QB).astype(f32)
-        ids = jnp.zeros((PEERS, 128), f32)
+        spot = lanes_of((LAYERS, 128))
+        for n in range(COLUMNS):
+            code = code_ref[n]
+            ids = jnp.zeros((LAYERS, 128), f32)
+            for s in range(CAP):
+                value = jnp.sum(jnp.where(mine & (code == float(s)), inner, 0.0), 1, keepdims=True)
+                ids = jnp.where(spot == s, value, ids)
+            ids_ref[n * LAYERS : (n + 1) * LAYERS, :] = ids.astype(jnp.int32)
+        copy = pltpu.make_async_copy(ids_ref, ids_smem, sem)
+        copy.start()
+        far_ref[:SPLIT, :] = far_a_ref[...]
+        far_ref[SPLIT:, :] = far_b_ref[...]
+        for d, ref in enumerate(stock):
+            column_ref[(place - d + LAYERS) % LAYERS] = ref[TOK:, :]
+        copy.wait()
+
+    for d, ref in enumerate(stock):
+        layer = (place - d + LAYERS) % LAYERS
         for s in range(CAP):
-            value = jnp.sum(jnp.where(mine & (codes == float(s)), inner, 0.0), 1, keepdims=True)
-            ids = jnp.where(lane == s, value, ids)
-        ids_ref[...] = ids.astype(jnp.int32)
-        copy = pltpu.make_async_copy(ids_ref, ids_smem, sems.at[1])
-        copy.start()
-        load.wait()
-        copy.wait()
-
-    for peer in range(PICK):
-        for s in range(CAP):
-            start = pl.multiple_of(ids_smem[step * PICK + peer, s] * BLK, BLK)
-            picked_ref[peer, s * BLK : (s + 1) * BLK, :] = pair_ref[pl.ds(start, BLK), :]
+            start = pl.multiple_of(ids_smem[asker * LAYERS + layer, s] * BLK, BLK)
+            row = pl.multiple_of((layer * CAP + s) * BLK, BLK)
+            picked_ref[0, pl.ds(row, BLK), :] = ref[pl.ds(start, BLK), :]
 
 
 def mixed_heads(result, gates, first):
@@ -263,16 +279,19 @@
 
 
 def compressed_kernel(
-    arrived_ref, query_ref, gates_ref, outk_ref, outv_ref, turn_ref, mixed_ref,
-    key_ref, value_ref, score_ref, weight_ref,
+    column0_ref, column1_ref, column2_ref, column3_ref, query_ref, gates_ref, outk_ref, outv_ref,
+    turn_ref, mixed_ref, arrived_ref, key_ref, value_ref, score_ref, weight_ref,
 ):
-    rank = lax.axis_index("kv")
+    rank = kv_index()
+    column = lax.axis_index("x")
+    for d, ref in enumerate((column0_ref, column1_ref, column2_ref, column3_ref)):
+        arrived_ref[(column - d + COLUMNS) % COLUMNS] = ref[...]
     flat = arrived_ref[...].reshape(PEERS * ROWS, 128)
     shape = (4 * PEERS, PEERS * ROWS)
     row = rows_of(shape)
     kind = row // PEERS
     source = row % PEERS + kind % 2
-    target = source * ROWS + NSUM + jnp.where(kind == 0, 0, jnp.where(kind == 1, 2, jnp.where(kind == 2, 1, 3)))
+    target = (source % COLUMNS * LAYERS + source // COLUMNS) * ROWS + NSUM + jnp.where(kind == 0, 0, jnp.where(kind == 1, 2, jnp.where(kind == 2, 1, 3)))
     edges = dot(((lanes_of(shape) == target) & (source < PEERS)).astype(bf16), flat)
     pre_k = edges[:PEERS] + edges[PEERS : 2 * PEERS]
     pre_v = edges[2 * PEERS : 3 * PEERS] + edges[3 * PEERS :]
@@ -281,7 +300,7 @@
     is_last = rows_of((NSUM, 128)) == NSUM - 1
     lane = lanes_of((NSUM, 128))
     for peer in range(PEERS):
-        chunk = arrived_ref[peer, :NSUM, :].astype(f32)
+        chunk = arrived_ref[peer % COLUMNS, peer // COLUMNS, :NSUM, :].astype(f32)
         chunk = jnp.where(is_last, last[peer : peer + 1], chunk)
         value_ref[peer * NSUM : (peer + 1) * NSUM, :] = jnp.where(lane < HD, 1.0, chunk).astype(bf16)
         key_ref[peer * NSUM : (peer + 1) * NSUM, :] = chunk.astype(bf16)
@@ -331,7 +350,7 @@
     copies = [
         (place_hbm, place_ref),
         (fetched_hbm, fetched_ref),
-        (pair_hbm, pair_ref),
+        (pair_hbm.at[pl.ds(0, TOK)], pair_ref),
         (query_hbm, query_ref),
         (bound_hbm, bound_ref),
         (gates_hbm, gates_ref),
@@ -395,16 +414,14 @@
 
 
 def output_kernel(
-    a0_ref, a1_ref, a2_ref, a3_ref, w0_ref, w1_ref, w2a_ref, w2b_ref, w3_ref,
+    a0_ref, a1_ref, a2_ref, a3_ref, w0_ref, w1_ref, w2_ref, w3_ref,
     mine_ref, other_ref, sum_ref,
 ):
     core = lax.axis_index("tp") % 2
     total = dot(a0_ref[...], w0_ref[...])
     total = total + dot(a1_ref[...], w1_ref[...])
     total = total + dot(a3_ref[...], w3_ref[...])
-    half = HEADS * HD // 2
-    total = total + dot(a2_ref[:, :half], w2a_ref[...])
-    total = total + dot(a2_ref[:, half:], w2b_ref[...])
+    total = total + dot(a2_ref[...], w2_ref[...])
     sum_ref[...] = total
     mine_ref[...] = sum_ref[pl.ds(pl.multiple_of(core * OUT_ROWS, OUT_ROWS), OUT_ROWS), :]
     other = pl.multiple_of((1 - core) * OUT_ROWS, OUT_ROWS)
@@ -432,14 +449,17 @@
     return pltpu.CompilerParams(vmem_limit_bytes=mib * 1024 * 1024)
 
 
+def across(value, distance):
+    return lax.ppermute(value, "z", [(i, (i + distance) % LAYERS) for i in range(LAYERS)])
+
+
+def along(value, distance):
+    return lax.ppermute(value, "x", [(i, (i + distance) % COLUMNS) for i in range(COLUMNS)])
+
+
 def around(value, distance):
     route = [(2 * y + c, 2 * ((y + distance) % CHIPS) + c) for y in range(CHIPS) for c in range(2)]
     return lax.ppermute(value, "tp", route)
-
-
-def tables(positions):
-    angles = positions.astype(f32)[:, None] * jnp.asarray(INVERSE_ROW)
-    return jnp.cos(angles), jnp.sin(angles) * jnp.asarray(SIGN_ROW)
 
 
 def on_device(
@@ -447,23 +467,26 @@
     summary_value_weight, squeeze_key_in, squeeze_key_out, squeeze_value_in, squeeze_value_out,
     gate_weight, output_weight, chosen_blocks,
 ):
-    kv_rank = lax.axis_index("kv")
     chosen = chosen_blocks[0]
-    chosen_key_t = chosen_key_weight.T
-    chosen_value_t = chosen_value_weight.T
     squeeze_key_t = squeeze_key_out.T
     squeeze_value_t = squeeze_value_out.T
-    gate_t = gate_weight.transpose(0, 2, 1)
     turn = jnp.asarray(np.concatenate([INVERSE_ROW, SIGN_ROW], 0))
-    payload, code = pl.pallas_call(
-        summary_kernel,
-        name="summaries",
-        out_shape=(shape_of((PEERS, ROWS, 128), bf16), stored((8, NBLK), f32)),
-        in_specs=[HBM] * 9,
-        out_specs=(VMEM, VMEM),
+    row_block = pl.BlockSpec((PART, 128), lambda n: (n, 0))
+    token_block = pl.BlockSpec((PART, 2048), lambda n: (n, 0))
+    payload, code, cosine, sine = pl.pallas_call(
+        token_kernel,
+        name="tokens",
+        out_shape=(
+            stored((TOK + ROWS, 128), bf16),
+            stored((8, NBLK), f32),
+            stored((TOK, 128), f32),
+            stored((TOK, 128), f32),
+        ),
+        in_specs=[HBM] * 11,
+        out_specs=(VMEM,) * 4,
         scratch_shapes=[
             pltpu.VMEM((TOK, 2048), bf16),
-            pltpu.VMEM((2 * HD, 2048), bf16),
+            pltpu.VMEM((4 * HD, 2048), bf16),
             pltpu.VMEM((2048, 128), bf16),
             pltpu.VMEM((2048, 128), bf16),
             pltpu.VMEM((HD, 128), bf16),
@@ -471,76 +494,81 @@
             pltpu.VMEM((2, 128), f32),
             pltpu.VMEM((QB, NSEL), jnp.int32),
             pltpu.VMEM((TOK, 128), f32),
-            pltpu.SemaphoreType.DMA((8 + CHUNKS,)),
+            pltpu.VMEM((2, TOK // 8, 128), f32),
+            pltpu.SemaphoreType.DMA((10 + CHUNKS,)),
         ],
-        compiler_params=limit(16),
+        compiler_params=limit(24),
         cost_estimate=pl.CostEstimate(flops=10**9, bytes_accessed=5 * 10**6, transcendentals=0),
     )(
         *far(
-            tokens, summary_key_weight.T, summary_value_weight.T, squeeze_key_in, squeeze_value_in,
-            squeeze_key_t, squeeze_value_t, turn, chosen,
+            tokens, summary_key_weight.T, summary_value_weight.T, chosen_key_weight.T,
+            chosen_value_weight.T, squeeze_key_in, squeeze_value_in, squeeze_key_t, squeeze_value_t,
+            turn, chosen,
         ),
     )
+    up2 = across(payload, 2)
+    down2 = across(payload, -2)
+    up1 = across(payload, 1)
+    down1 = across(payload, -1)
+    codes = [code] + [along(code, d) for d in range(1, COLUMNS)]
     weight_1 = around(output_weight, 1)
     weight_3 = around(output_weight, -1)
-    arrived = lax.all_to_all(payload, "kv", 0, 0, tiled=True)
-    cosine, sine = tables(kv_rank * TOK + jnp.arange(TOK, dtype=jnp.int32))
-    row_block = pl.BlockSpec((PART, 128), lambda n: (n, 0))
-    token_block = pl.BlockSpec((PART, 2048), lambda n: (n, 0))
-    pairs, gates = pl.pallas_call(
-        pair_kernel,
-        name="pairs",
-        out_shape=(stored((TOK, 128), bf16), stored((TOK, 2 * HEADS), f32)),
-        grid=(TOK // PART,),
-        in_specs=[token_block, VMEM, VMEM, VMEM, row_block, row_block],
-        out_specs=(row_block, pl.BlockSpec((PART, 2 * HEADS), lambda n: (n, 0))),
-        scratch_shapes=[pltpu.VMEM((2 * HD + 2 * HEADS, 2048), bf16)],
-        compiler_params=limit(16),
-        cost_estimate=pl.CostEstimate(flops=10**10, bytes_accessed=3 * 10**6, transcendentals=0),
-    )(*far(tokens, chosen_key_t, chosen_value_t), gate_t, *far(cosine, sine))
-    picked = pl.pallas_call(
-        pick_kernel,
-        name="pick",
-        out_shape=shape_of((PEERS, CAP * BLK, 128), bf16),
-        grid=(PEERS // PICK,),
-        in_specs=[VMEM, HBM],
-        out_specs=pl.BlockSpec((PICK, CAP * BLK, 128), lambda step: (step, 0, 0)),
-        scratch_shapes=[
-            pltpu.VMEM((TOK, 128), bf16),
-            pltpu.VMEM((PEERS, 128), jnp.int32),
-            pltpu.SMEM((PEERS, 128), jnp.int32),
-            pltpu.SemaphoreType.DMA((2,)),
-        ],
-        compiler_params=limit(8),
-    )(arrived, *far(pairs))
-    fetched = lax.all_to_all(picked, "kv", 0, 0, tiled=True)
-    queries, place, bound = pl.pallas_call(
+    far_a = across(up2[:SPLIT], 2)
+    far_b = across(down2[SPLIT:], -2)
+    up3 = across(up2, 1)
+    down3 = across(down2, -1)
+    queries, gates, place, bound = pl.pallas_call(
         query_kernel,
         name="queries",
         out_shape=(
             stored((QB, HEADS * BLK, 128), bf16),
+            stored((TOK, 2 * HEADS), f32),
             stored((QB, NSEL), jnp.int32),
             stored((QB, NSEL * BLK), f32),
         ),
         grid=(TOK // PART,),
         in_specs=[
-            token_block, VMEM, row_block, row_block, VMEM, VMEM,
+            token_block, VMEM, VMEM, row_block, row_block, VMEM, VMEM,
         ],
         out_specs=(
             pl.BlockSpec((PART // BLK, HEADS * BLK, 128), lambda n: (n, 0, 0)),
+            pl.BlockSpec((PART, 2 * HEADS), lambda n: (n, 0)),
             VMEM,
             VMEM,
         ),
         compiler_params=limit(16),
         cost_estimate=pl.CostEstimate(flops=10**10, bytes_accessed=3 * 10**6, transcendentals=0),
-    )(*far(tokens, query_weight, cosine, sine, chosen, code))
+    )(*far(tokens, query_weight), gate_weight.transpose(0, 2, 1), *far(cosine, sine, chosen, code))
+    picked, column = pl.pallas_call(
+        pick_kernel,
+        name="pick",
+        out_shape=(
+            stored((COLUMNS, LAYERS * CAP * BLK, 128), bf16),
+            stored((LAYERS, ROWS, 128), bf16),
+        ),
+        grid=(COLUMNS,),
+        in_specs=[VMEM] * (COLUMNS + 9),
+        out_specs=(pl.BlockSpec((1, LAYERS * CAP * BLK, 128), lambda n: (n, 0, 0)), VMEM),
+        scratch_shapes=[
+            pltpu.VMEM((TOK + ROWS, 128), bf16),
+            pltpu.VMEM((COLUMNS, 8, NBLK), f32),
+            pltpu.VMEM((PEERS, 128), jnp.int32),
+            pltpu.SMEM((PEERS, 128), jnp.int32),
+            pltpu.SemaphoreType.DMA,
+        ],
+        compiler_params=limit(8),
+    )(*far(code), *codes[1:], *far(payload), up1, up2, up3, far_a, far_b, down3, down2, down1)
+    fetched = lax.all_to_all(picked, "x", 0, 0, tiled=True)
+    columns = [column] + [along(column, d) for d in range(1, COLUMNS)]
+    weight_2 = around(weight_1, 1)
     mixed = pl.pallas_call(
         compressed_kernel,
         name="compressed",
         out_shape=stored((TOK, HEADS * HD), bf16),
-        in_specs=[VMEM] * 6,
+        in_specs=[VMEM] * (COLUMNS + 5),
         out_specs=VMEM,
         scratch_shapes=[
+            pltpu.VMEM((COLUMNS, LAYERS, ROWS, 128), bf16),
             pltpu.VMEM((PEERS * NSUM, 128), bf16),
             pltpu.VMEM((PEERS * NSUM, 128), bf16),
             pltpu.VMEM((QB * HEADS * BLK, PEERS * NSUM), f32),
@@ -548,11 +576,7 @@
         ],
         compiler_params=limit(24),
         cost_estimate=pl.CostEstimate(flops=10**10, bytes_accessed=3 * 10**6, transcendentals=0),
-    )(arrived, *far(queries, gates, squeeze_key_t, squeeze_value_t, turn))
-    weight_1, weight_3, mixed = lax.optimization_barrier((weight_1, weight_3, mixed))
-    half = weight_1.shape[0] // 2
-    weight_2a = around(weight_1[:half], 1)
-    weight_2b = around(weight_3[half:], -1)
+    )(*columns, *far(queries, gates, squeeze_key_t, squeeze_value_t, turn))
     pieces = pl.pallas_call(
         selected_kernel,
         name="selected",
@@ -576,7 +600,7 @@
         compiler_params=limit(24),
         cost_estimate=pl.CostEstimate(flops=10**9, bytes_accessed=3 * 10**6, transcendentals=0),
     )(
-        *far(place, fetched.reshape(PEERS * CAP * BLK, 128), pairs, queries, bound, gates, mixed),
+        *far(place, fetched.reshape(PEERS * CAP * BLK, 128), payload, queries, bound, gates, mixed),
     )
     piece_2 = around(pieces[2], 2)
     piece_1 = around(pieces[1], 1)
@@ -585,24 +609,25 @@
         output_kernel,
         name="output",
         out_shape=(shape_of((OUT_ROWS, 2048), f32), shape_of((OUT_ROWS, 2048), bf16)),
-        in_specs=[VMEM] * 9,
+        in_specs=[VMEM] * 8,
         out_specs=(VMEM, VMEM),
         scratch_shapes=[pltpu.VMEM((2 * OUT_ROWS, 2048), f32)],
         compiler_params=limit(16),
     )(
-        pieces[0], piece_1, piece_2, piece_3, output_weight, weight_1, weight_2a, weight_2b,
-        weight_3,
+        pieces[0], piece_1, piece_2, piece_3, output_weight, weight_1, weight_2, weight_3,
     )
     swapped = lax.ppermute(other, "tp", [(i, i ^ 1) for i in range(2 * CHIPS)])
     return (mine + swapped.astype(f32)).astype(bf16)
 
 
 def solution(mesh):
+    split = Mesh(mesh.devices.reshape(LAYERS, COLUMNS, 2 * CHIPS), ("z", "x", "tp"))
+    kv = ("z", "x")
     return jax.shard_map(
         on_device,
-        mesh=mesh,
+        mesh=split,
         in_specs=(
-            P("kv", None),
+            P(kv, None),
             P(None, "tp"),
             P(None, "tp"),
             P(None, "tp"),
@@ -614,8 +639,8 @@
             P(),
             P(None, None, "tp"),
             P("tp", None),
-            P("tp", "kv", None),
+            P("tp", kv, None),
         ),
-        out_specs=P(("kv", "tp"), None),
+        out_specs=P(("z", "x", "tp"), None),
         check_vma=False,
     )

time: 85.3 us -> 87.3 us (1.023)
  starting transfers between devices: 30.7 us -> 45.3 us
  waiting for transfers between devices: 18.9 us -> 10.6 us
  other arithmetic: 2.58 us -> 0.75 us
  local copies, waits for them, and re-layouts: 1.68 us -> 0.02 us
    ppermute x0 -> x14, starting transfers between devices: none -> 25.1 us  [the longest x8 16.7 us: across(): lax.ppermute(value, 'z', [(i, (i + distance) % LAYERS) for i in range(LAY...]
    all_to_all x2 -> x1, waiting for transfers between devices: 15.6 us -> 0.91 us  [on_device(): fetched = lax.all_to_all(picked, 'x', 0, 0, tiled=True)]
    all_to_all x2 -> x1, starting transfers between devices: 16.4 us -> 4.4 us  [on_device(): fetched = lax.all_to_all(picked, 'x', 0, 0, tiled=True)]
    ppermute x0 -> x14, waiting for transfers between devices: none -> 5.65 us  [the longest x6 3.73 us: along(): lax.ppermute(value, 'x', [(i, (i + distance) % COLUMNS) for i in range(CO...]
    ppermute x1, starting transfers between devices: 5.52 us -> 9.15 us  [on_device(): swapped = lax.ppermute(other, 'tp', [(i, i ^ 1) for i in range(2 * CHIPS)])]
    ppermute x7 -> x6, starting transfers between devices: 8.83 us -> 6.68 us  [around(): return lax.ppermute(value, 'tp', route)]
    mul x1 -> x0, other arithmetic: 1.83 us -> none  [tables(): return (jnp.cos(angles), jnp.sin(angles) * jnp.asarray(SIGN_ROW))]
    slice x2, local copies, waits for them, and re-layouts: 1.67 us -> 0.01 us  [the longest x1 0.01 us: on_device(): far_b = across(down2[SPLIT:], -2)]
  transfers between devices with their start and end apart: 10 -> 22, of which waited for: 6 -> 7; matrix products, arithmetic and copies ran while one was open for 4% -> 0% of each run, Pallas kernels for 34% -> 27%
where the time goes in v2:
time: 87.3 us; the launch traced here: 87 us
  starting transfers between devices  45.3 us (52%)
  Pallas kernels  30.2 us (35%)
  waiting for transfers between devices  10.6 us (12%)
    ppermute x8, starting transfers between devices, across(): lax.ppermute(value, 'z', [(i, (i + distance) % LAYERS) for i in range(LAY...  16.7 us
    ppermute x1, starting transfers between devices, on_device(): swapped = lax.ppermute(other, 'tp', [(i, i ^ 1) for i in range(2 * CHIPS)])  9.15 us
    pallas_call x1, Pallas kernels, on_device(): pl.pallas_call(compressed_kernel, name='compressed', out_shape=stored((TO...  8.75 us
    ppermute x6, starting transfers between devices, along(): lax.ppermute(value, 'x', [(i, (i + distance) % COLUMNS) for i in range(CO...  8.33 us
    ppermute x6, starting transfers between devices, around(): return lax.ppermute(value, 'tp', route)  6.68 us
    pallas_call x1, Pallas kernels, on_device(): pl.pallas_call(selected_kernel, name='selected', out_shape=(shape_of((PER...  5.74 us
    pallas_call x1, Pallas kernels, on_device(): pl.pallas_call(query_kernel, name='queries', out_shape=(stored((QB, HEADS...  5.25 us
    pallas_call x1, Pallas kernels, on_device(): pl.pallas_call(token_kernel, name='tokens', out_shape=(stored((TOK + ROWS...  4.64 us
  transfers between devices with their start and end apart: 22, of which 7 were waited for; matrix products, arithmetic and copies ran while one was open for 0% of the time, Pallas kernels for 27%

profile of v2, /device:TPU:1, one launch (start us, length us, event | category | flops | bytes accessed | tf_op | source)
XLA Modules:
  0.0 87.0 jit_solution(6339352548422226355)
XLA Ops:
  0.0 4.6 %tokens.1 = (bf16[552,128]{1,0:T(8,128)(2,1)}, f32[8,512]{1,0:T(8,128)}, f32[512,128]{1,0:T(8,128)}, f32[512,128]{1,0:T(8,128)}) custom-call(bf16[512,2048]{1,0:T(8,128)(2,1)} %tokens_ref.1, bf16[64,2048]{1,0:T(8,128)(2,1)} %bitcast.10, bf16[64,2048]{1,0:T(8,128)(2,1)} %bitcast.11, bf16[64,2048]{1,0:T(8,128)(2,1)} %bitcast.12, bf16[64,2048]{1,0:T(8,128)(2,1)} %bitcast.13, ...), custom_call_target="tpu_custom_call" | custom-call | flops 1000000000 | bytes 5000000 | tf_op jit(solution)/shard_map/tokens/pallas_call | solution.py:476
  4.7 6.9 %collective-permute-start.7 = (bf16[552,128]{1,0:T(8,128)(2,1)}, bf16[552,128]{1,0:T(8,128)(2,1)S(1)}, u32[]{:S(2)}, u32[]{:S(2)}) collective-permute-start(bf16[552,128]{1,0:T(8,128)(2,1)} %get-tuple-element.25.own_ref.pair_hbm), channel_id=1, source_target_pairs={{0,192},{32,224},{64,0},{96,32},{128,64},{160,96},{192,128},{224,1... | collective-permute-start | bytes 423944 | tf_op jit(solution)/shard_map/ppermute | solution.py:453
  11.6 3.1 %collective-permute-start.10 = (bf16[552,128]{1,0:T(8,128)(2,1)}, bf16[552,128]{1,0:T(8,128)(2,1)S(1)}, u32[]{:S(2)}, u32[]{:S(2)}) collective-permute-start(bf16[552,128]{1,0:T(8,128)(2,1)} %get-tuple-element.25.own_ref.pair_hbm), channel_id=1, source_target_pairs={{0,224},{32,0},{64,32},{96,64},{128,96},{160,128},{192,160},{224,1... | collective-permute-start | bytes 423944 | tf_op jit(solution)/shard_map/ppermute | solution.py:453
  14.7 2.5 %collective-permute-start.2 = (f32[8,512]{1,0:T(8,128)}, f32[8,512]{1,0:T(8,128)S(1)}, u32[]{:S(2)}, u32[]{:S(2)}) collective-permute-start(f32[8,512]{1,0:T(8,128)} %get-tuple-element.23.code_ref.code0_ref), channel_id=1, source_target_pairs={{0,24},{8,0},{16,8},{24,16},{1,25},{9,1},{17,9},{25,17},{2,26},{10... | collective-permute-start | bytes 49160 | tf_op jit(solution)/shard_map/ppermute | solution.py:457
  17.2 1.1 %collective-permute-done.2.code3_ref = f32[8,512]{1,0:T(8,128)S(1)} collective-permute-done((f32[8,512]{1,0:T(8,128)}, f32[8,512]{1,0:T(8,128)S(1)}, u32[]{:S(2)}, u32[]{:S(2)}) %collective-permute-start.2) | collective-permute-done | bytes 16416 | tf_op jit(solution)/shard_map/ppermute | solution.py:457
  18.3 2.0 %collective-permute-start.1 = (f32[8,512]{1,0:T(8,128)}, f32[8,512]{1,0:T(8,128)S(1)}, u32[]{:S(2)}, u32[]{:S(2)}) collective-permute-start(f32[8,512]{1,0:T(8,128)} %get-tuple-element.23.code_ref.code0_ref), channel_id=1, source_target_pairs={{0,16},{8,24},{16,0},{24,8},{1,17},{9,25},{17,1},{25,9},{2,18},{10... | collective-permute-start | bytes 49160 | tf_op jit(solution)/shard_map/ppermute | solution.py:457
  20.3 3.0 %collective-permute-start.9 = (bf16[552,128]{1,0:T(8,128)(2,1)S(1)}, bf16[552,128]{1,0:T(8,128)(2,1)S(1)}, u32[]{:S(2)}, u32[]{:S(2)}) collective-permute-start(bf16[552,128]{1,0:T(8,128)(2,1)S(1)} %collective-permute-done.7.down2_ref), channel_id=1, source_target_pairs={{0,224},{32,0},{64,32},{96,64},{128,96},{160,128},{192,160},{224,1... | collective-permute-start | bytes 423944 | tf_op jit(solution)/shard_map/ppermute | solution.py:453
  23.2 1.4 %collective-permute-start = (f32[8,512]{1,0:T(8,128)}, f32[8,512]{1,0:T(8,128)S(1)}, u32[]{:S(2)}, u32[]{:S(2)}) collective-permute-start(f32[8,512]{1,0:T(8,128)} %get-tuple-element.23.code_ref.code0_ref), channel_id=1, source_target_pairs={{0,8},{8,16},{16,24},{24,0},{1,9},{9,17},{17,25},{25,1},{2,10},{10... | collective-permute-start | bytes 49160 | tf_op jit(solution)/shard_map/ppermute | solution.py:457
  24.7 2.6 %collective-permute-done.code1_ref = f32[8,512]{1,0:T(8,128)S(1)} collective-permute-done((f32[8,512]{1,0:T(8,128)}, f32[8,512]{1,0:T(8,128)S(1)}, u32[]{:S(2)}, u32[]{:S(2)}) %collective-permute-start) | collective-permute-done | bytes 16416 | tf_op jit(solution)/shard_map/ppermute | solution.py:457
  27.3 1.3 %collective-permute-start.17 = (bf16[256,2048]{1,0:T(8,128)(2,1)S(1)}, bf16[256,2048]{1,0:T(8,128)(2,1)S(1)}, u32[]{:S(2)}, u32[]{:S(2)}) collective-permute-start(bf16[256,2048]{1,0:T(8,128)(2,1)S(1)} %copy-done), channel_id=1, source_target_pairs={{0,2},{1,3},{2,4},{3,5},{4,6},{5,7},{6,0},{7,1},{8,10},{9,11},{10,... | collective-permute-start | bytes 3145736 | tf_op jit(solution)/shard_map/ppermute | solution.py:462
  28.7 3.6 %collective-permute-start.8 = (bf16[264,128]{1,0:T(8,128)(2,1)S(1)}, bf16[264,128]{1,0:T(8,128)(2,1)S(1)}, u32[]{:S(2)}, u32[]{:S(2)}) collective-permute-start(bf16[264,128]{1,0:T(8,128)(2,1)S(1)} %slice.9), channel_id=1, source_target_pairs={{0,192},{32,224},{64,0},{96,32},{128,64},{160,96},{192,128},{224,1... | collective-permute-start | bytes 202760 | tf_op jit(solution)/shard_map/ppermute | solution.py:453
  32.4 1.9 %collective-permute-done.8.far_b_ref = bf16[264,128]{1,0:T(8,128)(2,1)S(1)} collective-permute-done((bf16[264,128]{1,0:T(8,128)(2,1)S(1)}, bf16[264,128]{1,0:T(8,128)(2,1)S(1)}, u32[]{:S(2)}, u32[]{:S(2)}) %collective-permute-start.8) | collective-permute-done | bytes 67616 | tf_op jit(solution)/shard_map/ppermute | solution.py:453
  34.3 1.4 %collective-permute-start.19 = (bf16[256,2048]{1,0:T(8,128)(2,1)S(1)}, bf16[256,2048]{1,0:T(8,128)(2,1)S(1)}, u32[]{:S(2)}, u32[]{:S(2)}) collective-permute-start(bf16[256,2048]{1,0:T(8,128)(2,1)S(1)} %copy-done), channel_id=1, source_target_pairs={{0,6},{1,7},{2,0},{3,1},{4,2},{5,3},{6,4},{7,5},{8,14},{9,15},{10,... | collective-permute-start | bytes 3145736 | tf_op jit(solution)/shard_map/ppermute | solution.py:462
  35.7 3.7 %pick.1 = (bf16[4,1024,128]{2,1,0:T(8,128)(2,1)}, bf16[8,40,128]{2,1,0:T(8,128)(2,1)}) custom-call(f32[8,512]{1,0:T(8,128)} %get-tuple-element.23.code_ref.code0_ref, f32[8,512]{1,0:T(8,128)S(1)} %collective-permute-done.code1_ref, f32[8,512]{1,0:T(8,128)S(1)} %collective-permute-done.1.code2_ref, f32[8,512]{1,0:T(8,128)S(1)} %collective-permute-done.2.code3_ref, ...), custom_call_target="tpu_custom_call" | custom-call | tf_op jit(solution)/shard_map/pick/pallas_call | solution.py:542
  39.5 1.7 %collective-permute-start.13 = (bf16[8,40,128]{2,1,0:T(8,128)(2,1)}, bf16[8,40,128]{2,1,0:T(8,128)(2,1)S(1)}, u32[]{:S(2)}, u32[]{:S(2)}) collective-permute-start(bf16[8,40,128]{2,1,0:T(8,128)(2,1)} %get-tuple-element.30.column0_ref), channel_id=1, source_target_pairs={{0,24},{8,0},{16,8},{24,16},{1,25},{9,1},{17,9},{25,17},{2,26},{10... | collective-permute-start | bytes 245768 | tf_op jit(solution)/shard_map/ppermute | solution.py:457
  41.2 0.5 collective-permute-start.12
  41.7 0.2 collective-permute-start.11
  41.9 5.2 %queries.1 = (bf16[16,128,128]{2,1,0:T(8,128)(2,1)}, f32[512,8]{1,0:T(8,128)}, s32[16,16]{1,0:T(8,128)}, f32[16,512]{1,0:T(8,128)}) custom-call(bf16[512,2048]{1,0:T(8,128)(2,1)} %tokens_ref.1, bf16[2048,256]{1,0:T(8,128)(2,1)} %wq_ref.1, bf16[2,4,2048]{2,1,0:T(4,128)(2,1)S(1)} %bitcast.9, f32[512,128]{1,0:T(8,128)} %get-tuple-element.21.cos_ref, ...), custom_call_target="tpu_custom_call" | custom-call | flops 10000000000 | bytes 3000000 | tf_op jit(solution)/shard_map/queries/pallas_call | solution.py:520
  47.2 4.4 %all-to-all-start = ((bf16[4,1024,128]{2,1,0:T(8,128)(2,1)}), bf16[4,1024,128]{2,1,0:T(8,128)(2,1)}, u32[]{:S(2)}, u32[]{:S(2)}) async-start(bf16[4,1024,128]{2,1,0:T(8,128)(2,1)} %get-tuple-element.26), calls=%async_computation | async-start | bytes 2097152 | tf_op jit(solution)/shard_map/all_to_all | solution.py:561
  51.6 0.1 collective-permute-start.18
  51.7 8.7 %compressed.1.mixed_hbm = bf16[512,256]{1,0:T(8,128)(2,1)} custom-call(bf16[8,40,128]{2,1,0:T(8,128)(2,1)S(1)} %copy-done.1, bf16[8,40,128]{2,1,0:T(8,128)(2,1)S(1)} %collective-permute-done.11.column1_ref, bf16[8,40,128]{2,1,0:T(8,128)(2,1)S(1)} %collective-permute-done.12.column2_ref, bf16[8,40,128]{2,1,0:T(8,128)(2,1)S(1)} %collective-permute-done.13.column3_ref, ...), custom_call_target="tpu_custom_call" | custom-call | flops 10000000000 | bytes 3000000 | tf_op jit(solution)/shard_map/compressed/pallas_call | solution.py:564
  60.5 0.9 %all-to-all-done = bf16[4,1024,128]{2,1,0:T(8,128)(2,1)} async-done(((bf16[4,1024,128]{2,1,0:T(8,128)(2,1)}), bf16[4,1024,128]{2,1,0:T(8,128)(2,1)}, u32[]{:S(2)}, u32[]{:S(2)}) %all-to-all-start) | async-done | bytes 1048608 | tf_op jit(solution)/shard_map/all_to_all | solution.py:561
  61.4 5.7 %selected.1 = (bf16[128,256]{1,0:T(8,128)(2,1)S(1)}, bf16[128,256]{1,0:T(8,128)(2,1)S(1)}, bf16[128,256]{1,0:T(8,128)(2,1)S(1)}, bf16[128,256]{1,0:T(8,128)(2,1)S(1)}) custom-call(s32[16,16]{1,0:T(8,128)} %get-tuple-element.24.place_hbm, bf16[4096,128]{1,0:T(8,128)(2,1)} %bitcast.8.fetched_hbm, bf16[552,128]{1,0:T(8,128)(2,1)} %get-tuple-element.25.own_ref.pair_hbm, ...), custom_call_target="tpu_custom_call" | custom-call | flops 1000000000 | bytes 3000000 | tf_op jit(solution)/shard_map/selected/pallas_call | solution.py:580
  67.1 0.4 collective-permute-start.14
  67.6 2.6 %collective-permute-start.15 = (bf16[128,256]{1,0:T(8,128)(2,1)S(1)}, bf16[128,256]{1,0:T(8,128)(2,1)S(1)}, u32[]{:S(2)}, u32[]{:S(2)}) collective-permute-start(bf16[128,256]{1,0:T(8,128)(2,1)S(1)} %get-tuple-element.33), channel_id=1, source_target_pairs={{0,4},{1,5},{2,6},{3,7},{4,0},{5,1},{6,2},{7,3},{8,12},{9,13},{10,... | collective-permute-start | bytes 196616 | tf_op jit(solution)/shard_map/ppermute | solution.py:462
  70.1 0.8 collective-permute-start.16
  71.0 1.7 %collective-permute-done.14.a1_ref = bf16[128,256]{1,0:T(8,128)(2,1)S(1)} collective-permute-done((bf16[128,256]{1,0:T(8,128)(2,1)S(1)}, bf16[128,256]{1,0:T(8,128)(2,1)S(1)}, u32[]{:S(2)}, u32[]{:S(2)}) %collective-permute-start.14) | collective-permute-done | bytes 65568 | tf_op jit(solution)/shard_map/ppermute | solution.py:462
  72.6 1.3 %collective-permute-done.15.a2_ref = bf16[128,256]{1,0:T(8,128)(2,1)S(1)} collective-permute-done((bf16[128,256]{1,0:T(8,128)(2,1)S(1)}, bf16[128,256]{1,0:T(8,128)(2,1)S(1)}, u32[]{:S(2)}, u32[]{:S(2)}) %collective-permute-start.15) | collective-permute-done | bytes 65568 | tf_op jit(solution)/shard_map/ppermute | solution.py:462
  73.9 2.0 %output.1 = (f32[64,2048]{1,0:T(8,128)S(1)}, bf16[64,2048]{1,0:T(8,128)(2,1)S(1)}) custom-call(bf16[128,256]{1,0:T(8,128)(2,1)S(1)} %get-tuple-element.31.a0_ref, bf16[128,256]{1,0:T(8,128)(2,1)S(1)} %collective-permute-done.14.a1_ref, bf16[128,256]{1,0:T(8,128)(2,1)S(1)} %collective-permute-done.15.a2_ref, ...), custom_call_target="tpu_custom_call" | custom-call | tf_op jit(solution)/shard_map/output/pallas_call | solution.py:608
  75.9 9.1 %collective-permute-start.20 = (bf16[64,2048]{1,0:T(8,128)(2,1)S(1)}, bf16[64,2048]{1,0:T(8,128)(2,1)S(1)}, u32[]{:S(2)}, u32[]{:S(2)}) collective-permute-start(bf16[64,2048]{1,0:T(8,128)(2,1)S(1)} %get-tuple-element.36), channel_id=1, source_target_pairs={{0,1},{1,0},{2,3},{3,2},{4,5},{5,4},{6,7},{7,6},{8,9},{9,8},{10,11... | collective-permute-start | bytes 786440 | tf_op jit(solution)/shard_map/ppermute | solution.py:619
  85.1 1.2 %collective-permute-done.20 = bf16[64,2048]{1,0:T(8,128)(2,1)S(1)} collective-permute-done((bf16[64,2048]{1,0:T(8,128)(2,1)S(1)}, bf16[64,2048]{1,0:T(8,128)(2,1)S(1)}, u32[]{:S(2)}, u32[]{:S(2)}) %collective-permute-start.20) | collective-permute-done | bytes 262176 | tf_op jit(solution)/shard_map/ppermute | solution.py:619
  86.2 0.8 add_convert_fusion
  (27 shorter events, 0.2 us)
Async XLA Ops:
  0.0 27.3 %copy-start = (bf16[256,2048]{1,0:T(8,128)(2,1)S(1)}, bf16[256,2048]{1,0:T(8,128)(2,1)}, u32[]{:S(2)}) copy-start(bf16[256,2048]{1,0:T(8,128)(2,1)} %w0_ref.1) | copy-start | bytes 3145732
  0.0 41.9 %copy-start.2 = (bf16[2,2048,4]{1,2,0:T(4,128)(2,1)S(1)}, bf16[2,2048,4]{1,2,0:T(4,128)(2,1)}, u32[]{:S(2)}) copy-start(bf16[2,2048,4]{1,2,0:T(4,128)(2,1)} %param.24) | copy-start | bytes 98308
  4.7 15.6 %collective-permute-start.7 = (bf16[552,128]{1,0:T(8,128)(2,1)}, bf16[552,128]{1,0:T(8,128)(2,1)S(1)}, u32[]{:S(2)}, u32[]{:S(2)}) collective-permute-start(bf16[552,128]{1,0:T(8,128)(2,1)} %get-tuple-element.25.own_ref.pair_hbm), channel_id=1, source_target_pairs={{0,192},{32,224},{64,0},{96,32},{128,64},{160,96},{192,128},{224,1... | collective-permute-start | bytes 423944 | tf_op jit(solution)/shard_map/ppermute | solution.py:453
  11.6 11.7 %collective-permute-start.4 = (bf16[552,128]{1,0:T(8,128)(2,1)}, bf16[552,128]{1,0:T(8,128)(2,1)S(1)}, u32[]{:S(2)}, u32[]{:S(2)}) collective-permute-start(bf16[552,128]{1,0:T(8,128)(2,1)} %get-tuple-element.25.own_ref.pair_hbm), channel_id=1, source_target_pairs={{0,64},{32,96},{64,128},{96,160},{128,192},{160,224},{192,0},{224,... | collective-permute-start | bytes 423944 | tf_op jit(solution)/shard_map/ppermute | solution.py:453
  11.6 17.1 %collective-permute-start.10 = (bf16[552,128]{1,0:T(8,128)(2,1)}, bf16[552,128]{1,0:T(8,128)(2,1)S(1)}, u32[]{:S(2)}, u32[]{:S(2)}) collective-permute-start(bf16[552,128]{1,0:T(8,128)(2,1)} %get-tuple-element.25.own_ref.pair_hbm), channel_id=1, source_target_pairs={{0,224},{32,0},{64,32},{96,64},{128,96},{160,128},{192,160},{224,1... | collective-permute-start | bytes 423944 | tf_op jit(solution)/shard_map/ppermute | solution.py:453
  14.7 14.0 %collective-permute-start.3 = (bf16[552,128]{1,0:T(8,128)(2,1)}, bf16[552,128]{1,0:T(8,128)(2,1)S(1)}, u32[]{:S(2)}, u32[]{:S(2)}) collective-permute-start(bf16[552,128]{1,0:T(8,128)(2,1)} %get-tuple-element.25.own_ref.pair_hbm), channel_id=1, source_target_pairs={{0,32},{32,64},{64,96},{96,128},{128,160},{160,192},{192,224},{224... | collective-permute-start | bytes 423944 | tf_op jit(solution)/shard_map/ppermute | solution.py:453
  14.7 3.6 %collective-permute-start.2 = (f32[8,512]{1,0:T(8,128)}, f32[8,512]{1,0:T(8,128)S(1)}, u32[]{:S(2)}, u32[]{:S(2)}) collective-permute-start(f32[8,512]{1,0:T(8,128)} %get-tuple-element.23.code_ref.code0_ref), channel_id=1, source_target_pairs={{0,24},{8,0},{16,8},{24,16},{1,25},{9,1},{17,9},{25,17},{2,26},{10... | collective-permute-start | bytes 49160 | tf_op jit(solution)/shard_map/ppermute | solution.py:457
  18.3 5.0 %collective-permute-start.1 = (f32[8,512]{1,0:T(8,128)}, f32[8,512]{1,0:T(8,128)S(1)}, u32[]{:S(2)}, u32[]{:S(2)}) collective-permute-start(f32[8,512]{1,0:T(8,128)} %get-tuple-element.23.code_ref.code0_ref), channel_id=1, source_target_pairs={{0,16},{8,24},{16,0},{24,8},{1,17},{9,25},{17,1},{25,9},{2,18},{10... | collective-permute-start | bytes 49160 | tf_op jit(solution)/shard_map/ppermute | solution.py:457
  20.3 15.5 %collective-permute-start.9 = (bf16[552,128]{1,0:T(8,128)(2,1)S(1)}, bf16[552,128]{1,0:T(8,128)(2,1)S(1)}, u32[]{:S(2)}, u32[]{:S(2)}) collective-permute-start(bf16[552,128]{1,0:T(8,128)(2,1)S(1)} %collective-permute-done.7.down2_ref), channel_id=1, source_target_pairs={{0,224},{32,0},{64,32},{96,64},{128,96},{160,128},{192,160},{224,1... | collective-permute-start | bytes 423944 | tf_op jit(solution)/shard_map/ppermute | solution.py:453
  23.2 12.5 %collective-permute-start.5 = (bf16[552,128]{1,0:T(8,128)(2,1)S(1)}, bf16[552,128]{1,0:T(8,128)(2,1)S(1)}, u32[]{:S(2)}, u32[]{:S(2)}) collective-permute-start(bf16[552,128]{1,0:T(8,128)(2,1)S(1)} %collective-permute-done.4.up2_ref), channel_id=1, source_target_pairs={{0,32},{32,64},{64,96},{96,128},{128,160},{160,192},{192,224},{224... | collective-permute-start | bytes 423944 | tf_op jit(solution)/shard_map/ppermute | solution.py:453
  23.2 4.1 %collective-permute-start = (f32[8,512]{1,0:T(8,128)}, f32[8,512]{1,0:T(8,128)S(1)}, u32[]{:S(2)}, u32[]{:S(2)}) collective-permute-start(f32[8,512]{1,0:T(8,128)} %get-tuple-element.23.code_ref.code0_ref), channel_id=1, source_target_pairs={{0,8},{8,16},{16,24},{24,0},{1,9},{9,17},{17,25},{25,1},{2,10},{10... | collective-permute-start | bytes 49160 | tf_op jit(solution)/shard_map/ppermute | solution.py:457
  27.3 24.3 %collective-permute-start.17 = (bf16[256,2048]{1,0:T(8,128)(2,1)S(1)}, bf16[256,2048]{1,0:T(8,128)(2,1)S(1)}, u32[]{:S(2)}, u32[]{:S(2)}) collective-permute-start(bf16[256,2048]{1,0:T(8,128)(2,1)S(1)} %copy-done), channel_id=1, source_target_pairs={{0,2},{1,3},{2,4},{3,5},{4,6},{5,7},{6,0},{7,1},{8,10},{9,11},{10,... | collective-permute-start | bytes 3145736 | tf_op jit(solution)/shard_map/ppermute | solution.py:462
  28.6 7.1 %collective-permute-start.6 = (bf16[288,128]{1,0:T(8,128)(2,1)S(1)}, bf16[288,128]{1,0:T(8,128)(2,1)S(1)}, u32[]{:S(2)}, u32[]{:S(2)}) collective-permute-start(bf16[288,128]{1,0:T(8,128)(2,1)S(1)} %slice.8), channel_id=1, source_target_pairs={{0,64},{32,96},{64,128},{96,160},{128,192},{160,224},{192,0},{224,... | collective-permute-start | bytes 221192 | tf_op jit(solution)/shard_map/ppermute | solution.py:453
  28.7 5.5 %collective-permute-start.8 = (bf16[264,128]{1,0:T(8,128)(2,1)S(1)}, bf16[264,128]{1,0:T(8,128)(2,1)S(1)}, u32[]{:S(2)}, u32[]{:S(2)}) collective-permute-start(bf16[264,128]{1,0:T(8,128)(2,1)S(1)} %slice.9), channel_id=1, source_target_pairs={{0,192},{32,224},{64,0},{96,32},{128,64},{160,96},{192,128},{224,1... | collective-permute-start | bytes 202760 | tf_op jit(solution)/shard_map/ppermute | solution.py:453
  34.3 36.7 %collective-permute-start.19 = (bf16[256,2048]{1,0:T(8,128)(2,1)S(1)}, bf16[256,2048]{1,0:T(8,128)(2,1)S(1)}, u32[]{:S(2)}, u32[]{:S(2)}) collective-permute-start(bf16[256,2048]{1,0:T(8,128)(2,1)S(1)} %copy-done), channel_id=1, source_target_pairs={{0,6},{1,7},{2,0},{3,1},{4,2},{5,3},{6,4},{7,5},{8,14},{9,15},{10,... | collective-permute-start | bytes 3145736 | tf_op jit(solution)/shard_map/ppermute | solution.py:462
  39.5 12.2 %collective-permute-start.13 = (bf16[8,40,128]{2,1,0:T(8,128)(2,1)}, bf16[8,40,128]{2,1,0:T(8,128)(2,1)S(1)}, u32[]{:S(2)}, u32[]{:S(2)}) collective-permute-start(bf16[8,40,128]{2,1,0:T(8,128)(2,1)} %get-tuple-element.30.column0_ref), channel_id=1, source_target_pairs={{0,24},{8,0},{16,8},{24,16},{1,25},{9,1},{17,9},{25,17},{2,26},{10... | collective-permute-start | bytes 245768 | tf_op jit(solution)/shard_map/ppermute | solution.py:457
  41.2 10.5 %collective-permute-start.12 = (bf16[8,40,128]{2,1,0:T(8,128)(2,1)}, bf16[8,40,128]{2,1,0:T(8,128)(2,1)S(1)}, u32[]{:S(2)}, u32[]{:S(2)}) collective-permute-start(bf16[8,40,128]{2,1,0:T(8,128)(2,1)} %get-tuple-element.30.column0_ref), channel_id=1, source_target_pairs={{0,16},{8,24},{16,0},{24,8},{1,17},{9,25},{17,1},{25,9},{2,18},{10... | collective-permute-start | bytes 245768 | tf_op jit(solution)/shard_map/ppermute | solution.py:457
  41.7 10.0 %collective-permute-start.11 = (bf16[8,40,128]{2,1,0:T(8,128)(2,1)}, bf16[8,40,128]{2,1,0:T(8,128)(2,1)S(1)}, u32[]{:S(2)}, u32[]{:S(2)}) collective-permute-start(bf16[8,40,128]{2,1,0:T(8,128)(2,1)} %get-tuple-element.30.column0_ref), channel_id=1, source_target_pairs={{0,8},{8,16},{16,24},{24,0},{1,9},{9,17},{17,25},{25,1},{2,10},{10... | collective-permute-start | bytes 245768 | tf_op jit(solution)/shard_map/ppermute | solution.py:457
  47.2 4.5 %copy-start.1 = (bf16[8,40,128]{2,1,0:T(8,128)(2,1)S(1)}, bf16[8,40,128]{2,1,0:T(8,128)(2,1)}, u32[]{:S(2)}) copy-start(bf16[8,40,128]{2,1,0:T(8,128)(2,1)} %get-tuple-element.30.column0_ref) | copy-start | bytes 245764
  47.2 14.2 %all-to-all-start = ((bf16[4,1024,128]{2,1,0:T(8,128)(2,1)}), bf16[4,1024,128]{2,1,0:T(8,128)(2,1)}, u32[]{:S(2)}, u32[]{:S(2)}) async-start(bf16[4,1024,128]{2,1,0:T(8,128)(2,1)} %get-tuple-element.26), calls=%async_computation | async-start | bytes 2097152 | tf_op jit(solution)/shard_map/all_to_all | solution.py:561
  51.6 22.3 %collective-permute-start.18 = (bf16[256,2048]{1,0:T(8,128)(2,1)S(1)}, bf16[256,2048]{1,0:T(8,128)(2,1)}, u32[]{:S(2)}, u32[]{:S(2)}) collective-permute-start(bf16[256,2048]{1,0:T(8,128)(2,1)S(1)} %collective-permute-done.17.w1_ref), channel_id=1, source_target_pairs={{0,2},{1,3},{2,4},{3,5},{4,6},{5,7},{6,0},{7,1},{8,10},{9,11},{10,... | collective-permute-start | bytes 3145736 | tf_op jit(solution)/shard_map/ppermute | solution.py:462
  67.1 5.5 %collective-permute-start.14 = (bf16[128,256]{1,0:T(8,128)(2,1)S(1)}, bf16[128,256]{1,0:T(8,128)(2,1)S(1)}, u32[]{:S(2)}, u32[]{:S(2)}) collective-permute-start(bf16[128,256]{1,0:T(8,128)(2,1)S(1)} %get-tuple-element.32), channel_id=1, source_target_pairs={{0,2},{1,3},{2,4},{3,5},{4,6},{5,7},{6,0},{7,1},{8,10},{9,11},{10,... | collective-permute-start | bytes 196616 | tf_op jit(solution)/shard_map/ppermute | solution.py:462
  67.6 6.3 %collective-permute-start.15 = (bf16[128,256]{1,0:T(8,128)(2,1)S(1)}, bf16[128,256]{1,0:T(8,128)(2,1)S(1)}, u32[]{:S(2)}, u32[]{:S(2)}) collective-permute-start(bf16[128,256]{1,0:T(8,128)(2,1)S(1)} %get-tuple-element.33), channel_id=1, source_target_pairs={{0,4},{1,5},{2,6},{3,7},{4,0},{5,1},{6,2},{7,3},{8,12},{9,13},{10,... | collective-permute-start | bytes 196616 | tf_op jit(solution)/shard_map/ppermute | solution.py:462
  70.1 3.8 %collective-permute-start.16 = (bf16[128,256]{1,0:T(8,128)(2,1)S(1)}, bf16[128,256]{1,0:T(8,128)(2,1)S(1)}, u32[]{:S(2)}, u32[]{:S(2)}) collective-permute-start(bf16[128,256]{1,0:T(8,128)(2,1)S(1)} %get-tuple-element.34), channel_id=1, source_target_pairs={{0,6},{1,7},{2,0},{3,1},{4,2},{5,3},{6,4},{7,5},{8,14},{9,15},{10,... | collective-permute-start | bytes 196616 | tf_op jit(solution)/shard_map/ppermute | solution.py:462
  75.9 10.3 %collective-permute-start.20 = (bf16[64,2048]{1,0:T(8,128)(2,1)S(1)}, bf16[64,2048]{1,0:T(8,128)(2,1)S(1)}, u32[]{:S(2)}, u32[]{:S(2)}) collective-permute-start(bf16[64,2048]{1,0:T(8,128)(2,1)S(1)} %get-tuple-element.36), channel_id=1, source_target_pairs={{0,1},{1,0},{2,3},{3,2},{4,5},{5,4},{6,7},{7,6},{8,9},{9,8},{10,11... | collective-permute-start | bytes 786440 | tf_op jit(solution)/shard_map/ppermute | solution.py:619
